TPU v7x, 32 devices: a whole 2x2x4 slice. The times are simulated.
32 devices in a mesh: sp: 8 (over z, x), tp: 4 (over y, core).
Axes of the slice: x: 2, y: 2, z: 4, core: 2. Of those that a mesh axis runs over, the one named last changes fastest.
Arguments:
- queries: bfloat16 [512, 1024], P('tp', 'sp'), may hold values from -6 to 6
- input_key_matrix: bfloat16 [512, 1024], P('tp', 'sp'), may hold values from -6 to 6
- input_value_matrix: bfloat16 [1024, 1024], P('tp', 'sp'), may hold values from -6 to 6
- decay_preactivation: bfloat16 [512, 1024], P('tp', 'sp'), may hold values from -6 to 6
- extra_log_decay: float32 [512, 1024], P('tp', 'sp'), may hold values from -1 to 0, as said below
- channel_decay_speed: float32 [512], P('tp'), may hold values from 0 to 1, as said below
- output_weight_matrix: bfloat16 [2048, 1024], P(None, 'tp'), may hold values from -0.1875 to 0.1875
- stored_expert_rows: bfloat16 [1024, 2048], P('sp', 'tp'), may hold values from -6 to 6
- chosen_expert_index: int32 [1024, 2], P('sp'), may hold values from 0 to 7, all different within a row; in each aligned block of 128 rows (0 to 127, 128 to 255, ...) at most 48 rows name the same one
- expert_combine_weight: float32 [1024, 2], P('sp'), may hold values from 0.2 to 1
- cotangent: bfloat16 [1024, 2048], P('sp', 'tp'), may hold values from -6 to 6
- expert_gate_weight: bfloat16 [8, 2048, 2048], P('sp', None, 'tp'), may hold values from -0.125 to 0.125
- expert_up_weight: bfloat16 [8, 2048, 2048], P('sp', None, 'tp'), may hold values from -0.125 to 0.125
- expert_down_weight: bfloat16 [8, 2048, 2048], P('sp', 'tp'), may hold values from -0.125 to 0.125
Outputs:
- grad_queries: float32 [512, 1024], P('tp', 'sp')
- grad_keys: float32 [512, 1024], P('tp', 'sp')
- grad_values: float32 [1024, 1024], P('tp', 'sp')
- grad_logit: float32 [512, 1024], P('tp', 'sp')
- grad_out_proj: float32 [2048, 1024], P('sp', 'tp')
- grad_gate: bfloat16 [8, 2048, 2048], P('sp', None, 'tp')
- grad_up: bfloat16 [8, 2048, 2048], P('sp', None, 'tp')
- grad_down: bfloat16 [8, 2048, 2048], P('sp', 'tp')
Inputs may be any that keep to these rules, and one draw needn't show every extreme that they name: `chosen_expert_index`: each position names two different experts; in the rows of one device no expert is named more than 48 times. `channel_decay_speed`: positive. `extra_log_decay`: zero or negative.
All inputs are finite; a program needn't handle non-finite values.
Results may differ from a plain program's by a relative error of at most 0.023.
Values may be sent and summed in bfloat16 or wider, within the bound.
A program may use at most 64 MiB of HBM per device.

v0:
```python
import functools

import jax
import jax.numpy as jnp
from jax import lax
from jax.experimental import pallas as pl
from jax.experimental.pallas import tpu as pltpu
from jax.sharding import PartitionSpec as P

KEY_DIM = 32
VAL_DIM = 64
BF16 = jnp.bfloat16
F32 = jnp.float32


def dot(a, b, contract):
    return lax.dot_general(a.astype(BF16), b.astype(BF16), (contract, ((), ())),
                           preferred_element_type=F32)


def exact_dot(a, b):
    return lax.dot_general(a, b, (((1,), (0,)), ((), ())), precision=lax.Precision.HIGHEST,
                           preferred_element_type=F32)


def triangle(length, test):
    rows = lax.broadcasted_iota(jnp.int32, (length, length), 0)
    cols = lax.broadcasted_iota(jnp.int32, (length, length), 1)
    return test(rows, cols)


def head_kernel(q_ref, k_ref, v_ref, pre_ref, extra_ref, speed_ref,
                st_ref, inner_ref, cum_ref, fwd_ref, bwd_ref):
    length = q_ref.shape[1]
    q = q_ref[...].astype(F32) * KEY_DIM ** (-0.5)
    k = k_ref[...].astype(F32)
    v = v_ref[...]
    pre = pre_ref[...].astype(F32)
    log_sig = jnp.minimum(pre, 0.0) - jnp.log1p(jnp.exp(-jnp.abs(pre)))
    decays = speed_ref[...] * log_sig + extra_ref[...]
    upto = triangle(length, lambda a, b: a <= b).astype(F32)
    cum = exact_dot(decays, upto)
    cum_ref[...] = cum
    cum_t = cum.T
    k_t = k.T
    total = jnp.zeros((length, length), F32)
    for c in range(KEY_DIM):
        weight = jnp.exp(-jnp.abs(cum_t[:, c:c + 1] - cum[c:c + 1, :]))
        total = total + (k_t[:, c:c + 1] * q[c:c + 1, :]) * weight
    scores = total.astype(BF16)
    st_ref[...] = scores
    inner_ref[...] = dot(v, scores, ((1,), (0,)))
    last = cum[:, length - 1:length]
    fwd = dot(k * jnp.exp(last - cum), v, ((1,), (1,)))
    bwd = dot(k * jnp.exp(cum), v, ((1,), (1,)))
    high = last.astype(BF16)
    rest = last - high.astype(F32)
    middle = rest.astype(BF16)
    low = (rest - middle.astype(F32)).astype(BF16)
    lane = lax.broadcasted_iota(jnp.int32, (KEY_DIM, VAL_DIM), 1)
    logs = jnp.where(lane == 0, high.astype(F32),
                     jnp.where(lane == 1, middle.astype(F32), low.astype(F32)))
    fwd_ref[...] = jnp.concatenate([fwd, logs], axis=1).astype(BF16)
    bwd_ref[...] = jnp.concatenate([bwd, logs], axis=1).astype(BF16)


def carry(recv, me, sums_of, factors):
    peers = recv.shape[0]
    zero = jnp.zeros((KEY_DIM, VAL_DIM), F32)
    before, after = zero, zero
    for i in range(peers):
        before = jnp.where(i < me, before * factors[i] + sums_of(i), before)
    for i in reversed(range(peers)):
        after = jnp.where(i > me, after * factors[i] + sums_of(i), after)
    return before, after


def factors_of(recv):
    out = []
    for i in range(recv.shape[0]):
        logs = recv[i, :, VAL_DIM:VAL_DIM + 3].astype(F32)
        out.append(jnp.exp(logs[:, 0:1] + logs[:, 1:2] + logs[:, 2:3]))
    return out


def mix_kernel(me_ref, recv_ref, q_ref, cum_ref, inner_ref,
               carried_ref, normed_ref, inv_ref, rows_ref):
    length = q_ref.shape[1]
    me = me_ref[0]
    fwd_in, bwd_in = carry(
        recv_ref, me, lambda i: recv_ref[i, :, :VAL_DIM].astype(F32), factors_of(recv_ref))
    carried_ref[...] = jnp.concatenate([fwd_in, bwd_in], axis=1)
    q = q_ref[...].astype(F32) * KEY_DIM ** (-0.5)
    cum = cum_ref[...]
    last = cum[:, length - 1:length]
    mixed = inner_ref[...] + dot(fwd_in, q * jnp.exp(cum), ((0,), (0,)))
    mixed = mixed + dot(bwd_in, q * jnp.exp(last - cum), ((0,), (0,)))
    inv = lax.rsqrt(jnp.mean(mixed * mixed, axis=0, keepdims=True) + 1e-06)
    normed = mixed * inv
    normed_ref[...] = normed
    inv_ref[...] = jnp.broadcast_to(inv, inv_ref.shape)
    rows_ref[...] = normed.astype(BF16)


def source_kernel(gn_ref, normed_ref, inv_ref, q_ref, cum_ref, dm_ref, fwd_ref, bwd_ref):
    length = q_ref.shape[1]
    normed = normed_ref[...]
    gn = gn_ref[...]
    dm = inv_ref[0:1, :] * (gn - normed * jnp.mean(gn * normed, axis=0, keepdims=True))
    dm_ref[...] = dm
    q = q_ref[...].astype(F32) * KEY_DIM ** (-0.5)
    cum = cum_ref[...]
    last = cum[:, length - 1:length]
    fwd = dot(q * jnp.exp(cum), dm, ((1,), (1,)))
    bwd = dot(q * jnp.exp(last - cum), dm, ((1,), (1,)))
    pad = jnp.zeros_like(fwd)
    fwd_ref[...] = jnp.concatenate([fwd, pad], axis=1).astype(BF16)
    bwd_ref[...] = jnp.concatenate([bwd, pad], axis=1).astype(BF16)


def inner_kernel(dm_ref, q_ref, k_ref, v_ref, cum_ref, st_ref, carried_ref,
                 dq_ref, dk_ref, dv_ref, dc_ref, dt_ref):
    length = q_ref.shape[1]
    dm = dm_ref[...]
    q = q_ref[...].astype(F32) * KEY_DIM ** (-0.5)
    k = k_ref[...].astype(F32)
    v = v_ref[...]
    cum = cum_ref[...]
    by_query = dot(dm, v, ((0,), (0,)))
    by_key = dot(v, dm, ((0,), (0,)))
    sign = jnp.where(triangle(length, lambda a, b: a > b), 1.0,
                     jnp.where(triangle(length, lambda a, b: a < b), -1.0, 0.0)).astype(F32)
    by_query_signed = by_query * sign
    by_key_signed = by_key * -sign
    cum_t, q_t, k_t = cum.T, q.T, k.T
    dq, dk, dq_signed, dk_signed = [], [], [], []
    for c in range(KEY_DIM):
        weight = jnp.exp(-jnp.abs(cum_t[:, c:c + 1] - cum[c:c + 1, :]))
        with_q = weight * q_t[:, c:c + 1]
        with_k = weight * k_t[:, c:c + 1]
        dk.append(jnp.sum(by_query * with_q, axis=0, keepdims=True))
        dk_signed.append(jnp.sum(by_query_signed * with_q, axis=0, keepdims=True))
        dq.append(jnp.sum(by_key * with_k, axis=0, keepdims=True))
        dq_signed.append(jnp.sum(by_key_signed * with_k, axis=0, keepdims=True))
    join = lambda rows: jnp.concatenate(rows, axis=0)
    last = cum[:, length - 1:length]
    carried = carried_ref[...]
    up, down = jnp.exp(cum), jnp.exp(last - cum)
    d_up = dot(carried[:, :VAL_DIM], dm, ((1,), (0,))) * up
    d_down = dot(carried[:, VAL_DIM:], dm, ((1,), (0,))) * down
    dq_ref[...] = (join(dq) + d_up + d_down) * KEY_DIM ** (-0.5)
    dk_ref[...] = join(dk)
    dv_ref[...] = dot(dm, st_ref[...], ((1,), (1,)))
    dc_ref[...] = q * (join(dq_signed) + d_up - d_down) - k * join(dk_signed)
    dt_ref[...] = jnp.broadcast_to(
        jnp.sum(q * d_down, axis=1, keepdims=True), dt_ref.shape)


def last_kernel(me_ref, recv_ref, first_ref, carried_ref, k_ref, v_ref, cum_ref,
                pre_ref, speed_ref, dk_in_ref, dv_in_ref, dc_in_ref, dt_ref,
                dk_ref, dv_ref, logit_ref):
    length = k_ref.shape[1]
    me = me_ref[0]
    grad_bwd, grad_fwd = carry(
        recv_ref, me, lambda i: recv_ref[i, :, :VAL_DIM].astype(F32), factors_of(first_ref))
    k = k_ref[...].astype(F32)
    v = v_ref[...]
    cum = cum_ref[...]
    last = cum[:, length - 1:length]
    up, down = jnp.exp(cum), jnp.exp(last - cum)
    d_down = dot(grad_fwd, v, ((1,), (0,))) * down
    d_up = dot(grad_bwd, v, ((1,), (0,))) * up
    dk_ref[...] = dk_in_ref[...] + d_down + d_up
    dv_ref[...] = (dv_in_ref[...] + dot(grad_fwd, k * down, ((0,), (0,)))
                   + dot(grad_bwd, k * up, ((0,), (0,))))
    carried = carried_ref[...]
    grad_factor = jnp.sum(grad_fwd * carried[:, :VAL_DIM] + grad_bwd * carried[:, VAL_DIM:],
                          axis=1, keepdims=True)
    grad_total = (dt_ref[:, 0:1] + jnp.sum(k * d_down, axis=1, keepdims=True)
                  + grad_factor * jnp.exp(last))
    dc = dc_in_ref[...] + k * (d_up - d_down)
    from_here = triangle(length, lambda a, b: a >= b).astype(F32)
    grad_decay = exact_dot(dc, from_here) + grad_total
    pre = pre_ref[...].astype(F32)
    logit_ref[...] = grad_decay * speed_ref[...] * jax.nn.sigmoid(-pre)


def per_head(kernel, heads, outs, args, vmem_ops, scalars=0):
    def spec(shape):
        if len(shape) == 3:
            return pl.BlockSpec((shape[0], shape[1] // heads, shape[2]), lambda h: (0, h, 0))
        return pl.BlockSpec((shape[0] // heads, shape[1]), lambda h: (h, 0))

    in_specs = [pl.BlockSpec(memory_space=pltpu.SMEM)] * scalars
    in_specs += [spec(arg.shape) for arg in args[scalars:]]
    return pl.pallas_call(
        kernel,
        grid=(heads,),
        in_specs=in_specs,
        out_specs=[spec(shape) for shape, _ in outs],
        out_shape=[jax.ShapeDtypeStruct(shape, dtype) for shape, dtype in outs],
        cost_estimate=pl.CostEstimate(
            flops=vmem_ops * heads, bytes_accessed=1 << 20, transcendentals=0),
        compiler_params=pltpu.CompilerParams(dimension_semantics=("arbitrary",)),
    )(*args)


def body(
    queries,
    input_key_matrix,
    input_value_matrix,
    decay_preactivation,
    extra_log_decay,
    channel_decay_speed,
    output_weight_matrix,
    stored_expert_rows,
    chosen_expert_index,
    expert_combine_weight,
    cotangent,
    expert_gate_weight,
    expert_up_weight,
    expert_down_weight,
):
    heads = input_value_matrix.shape[0] // VAL_DIM
    tok_rows = queries.shape[1]
    experts = lax.axis_size("sp")
    index = lax.axis_index("sp")
    me = index.astype(jnp.int32).reshape(1)
    capacity = 3 * tok_rows // experts
    slots = experts * capacity
    part_width = stored_expert_rows.shape[1]
    model_width = expert_gate_weight.shape[1]
    channels = heads * KEY_DIM
    values = heads * VAL_DIM
    tn = (((0,), (0,)), ((), ()))
    nt = (((1,), (1,)), ((), ()))

    expert_ids = lax.broadcasted_iota(jnp.int32, (tok_rows, experts), 1)
    picks = [chosen_expert_index[:, i:i + 1] == expert_ids for i in range(2)]
    earlier = triangle(tok_rows, lambda a, b: a > b).astype(BF16)
    counts = jnp.dot(earlier, (picks[0] | picks[1]).astype(BF16), preferred_element_type=F32)
    slot_ids = lax.broadcasted_iota(jnp.int32, (tok_rows, slots), 1)
    places = []
    for i in range(2):
        rank = jnp.sum(jnp.where(picks[i], counts, 0.0), axis=1, keepdims=True)
        slot = chosen_expert_index[:, i:i + 1] * capacity + rank.astype(jnp.int32)
        places.append((slot == slot_ids).astype(BF16))
    place = places[0] + places[1]
    weighted = [
        (expert_combine_weight[:, i:i + 1] * cotangent.astype(F32)).astype(BF16)
        for i in range(2)
    ]
    send_x = lax.dot_general(place, stored_expert_rows, tn, preferred_element_type=F32)
    send_dy = lax.dot_general(jnp.concatenate(places, axis=0), jnp.concatenate(weighted, axis=0),
                              tn, preferred_element_type=F32)

    def exchange(rows):
        rows = rows.astype(BF16).reshape(experts, capacity, part_width)
        rows = lax.all_to_all(rows, "sp", split_axis=0, concat_axis=0, tiled=True)
        return lax.all_gather(rows.reshape(slots, part_width), "tp", axis=1, tiled=True)

    rows_x = exchange(send_x)
    rows_dy = exchange(send_dy)

    speed = channel_decay_speed[:, None]
    state = ((channels, 2 * VAL_DIM), BF16)
    scores, inner, cum, fwd_sum, bwd_sum = per_head(
        head_kernel, heads,
        [((heads * tok_rows, tok_rows), BF16), ((values, tok_rows), F32),
         ((channels, tok_rows), F32), state, state],
        [queries, input_key_matrix, input_value_matrix, decay_preactivation, extra_log_decay,
         speed], 1 << 28)
    peer = lax.broadcasted_iota(jnp.int32, (experts, 1, 1), 0)
    gate_local = expert_gate_weight[0]
    up_local = expert_up_weight[0]
    gate_pre = jnp.dot(rows_x, gate_local, preferred_element_type=F32)
    up_pre = jnp.dot(rows_x, up_local, preferred_element_type=F32)
    rows_dy, fwd_sum, bwd_sum, gate_pre, up_pre = lax.optimization_barrier(
        (rows_dy, fwd_sum, bwd_sum, gate_pre, up_pre))
    sums = lax.all_to_all(jnp.where(peer > index, fwd_sum[None], bwd_sum[None]),
                          "sp", split_axis=0, concat_axis=0, tiled=True)
    carried, normed, inv_rms, mix_rows = per_head(
        mix_kernel, heads,
        [((channels, 2 * VAL_DIM), F32), ((values, tok_rows), F32), ((heads * 8, tok_rows), F32),
         ((values, tok_rows), BF16)],
        [me, sums, queries, cum, inner], 1 << 26, scalars=1)
    all_mix = lax.all_to_all(jnp.broadcast_to(mix_rows[None], (experts, values, tok_rows)),
                             "sp", split_axis=0, concat_axis=0, tiled=True)

    down_local = expert_down_weight[0]
    gate_sig = jax.nn.sigmoid(gate_pre)
    gate_act = gate_pre * gate_sig
    hidden = (gate_act * up_pre).astype(BF16)
    grad_hidden = lax.dot_general(rows_dy, down_local, nt, preferred_element_type=F32)
    grad_gate_pre = (grad_hidden * up_pre * gate_sig * (1.0 + gate_pre * (1.0 - gate_sig))).astype(
        BF16
    )
    grad_up_pre = (grad_hidden * gate_act).astype(BF16)
    partial_value = lax.dot_general(grad_gate_pre, gate_local, nt, preferred_element_type=F32)
    partial_value = partial_value + lax.dot_general(
        grad_up_pre, up_local, nt, preferred_element_type=F32
    )
    summed = lax.psum_scatter(
        partial_value.astype(BF16), "tp", scatter_dimension=1, tiled=True
    ).reshape(experts, capacity, part_width)
    grad_down = lax.dot_general(hidden, rows_dy, tn, preferred_element_type=F32).astype(BF16)
    grad_gate = lax.dot_general(rows_x, grad_gate_pre, tn, preferred_element_type=F32).astype(BF16)
    grad_up = lax.dot_general(rows_x, grad_up_pre, tn, preferred_element_type=F32).astype(BF16)
    summed, all_mix = lax.optimization_barrier((summed, all_mix))
    returned = lax.all_to_all(summed, "sp", split_axis=0, concat_axis=0, tiled=True)
    picked = jnp.dot(place, returned.reshape(slots, part_width), preferred_element_type=F32)
    grad_rows = (cotangent.astype(F32) + picked).astype(BF16)
    full_rows = lax.all_gather(grad_rows, "tp", axis=1, tiled=True)
    grad_normed = lax.dot_general(
        output_weight_matrix, full_rows, (((0,), (1,)), ((), ())), preferred_element_type=F32
    )
    grad_mixed, fwd_source, bwd_source = per_head(
        source_kernel, heads, [((values, tok_rows), F32), state, state],
        [grad_normed, normed, inv_rms, queries, cum], 1 << 26)
    sources = lax.all_to_all(jnp.where(peer < index, fwd_source[None], bwd_source[None]),
                             "sp", split_axis=0, concat_axis=0, tiled=True)
    by_channel = ((channels, tok_rows), F32)
    grad_queries, dk, dv, dc, dt = per_head(
        inner_kernel, heads,
        [by_channel, by_channel, ((values, tok_rows), F32), by_channel, by_channel],
        [grad_mixed, queries, input_key_matrix, input_value_matrix, cum, scores, carried],
        1 << 29)
    full_rows, dk = lax.optimization_barrier((full_rows, dk))
    rows_block = model_width // experts
    all_rows = lax.all_to_all(full_rows.reshape(tok_rows, experts, rows_block).swapaxes(0, 1),
                              "sp", split_axis=0, concat_axis=0, tiled=True)
    grad_out_proj = lax.dot_general(
        all_rows.reshape(experts * tok_rows, rows_block),
        all_mix.swapaxes(1, 2).reshape(experts * tok_rows, values),
        tn, preferred_element_type=F32)
    grad_keys, grad_values, grad_logit = per_head(
        last_kernel, heads, [by_channel, ((values, tok_rows), F32), by_channel],
        [me, sources, sums, carried, input_key_matrix, input_value_matrix, cum,
         decay_preactivation, speed, dk, dv, dc, dt], 1 << 26, scalars=1)
    return (
        grad_queries,
        grad_keys,
        grad_values,
        grad_logit,
        grad_out_proj,
        grad_gate[None],
        grad_up[None],
        grad_down[None],
    )


def solution(mesh):
    in_specs = (
        P("tp", "sp"),
        P("tp", "sp"),
        P("tp", "sp"),
        P("tp", "sp"),
        P("tp", "sp"),
        P("tp"),
        P(None, "tp"),
        P("sp", "tp"),
        P("sp", None),
        P("sp", None),
        P("sp", "tp"),
        P("sp", None, "tp"),
        P("sp", None, "tp"),
        P("sp", "tp", None),
    )
    out_specs = (
        P("tp", "sp"),
        P("tp", "sp"),
        P("tp", "sp"),
        P("tp", "sp"),
        P("sp", "tp"),
        P("sp", None, "tp"),
        P("sp", None, "tp"),
        P("sp", "tp", None),
    )
    return jax.shard_map(body, mesh=mesh, in_specs=in_specs, out_specs=out_specs, check_vma=False)
```

profile of v0, /device:TPU:0, one launch (start us, length us, event | category | flops | bytes accessed | tf_op | source)
XLA Modules:
  0.0 184.5 jit_solution(9091092912472847958)
XLA Ops:
  10.3 19.2 %all_to_all.35 = bf16[8,48,512]{2,1,0:T(8,128)(2,1)} all-to-all(bf16[8,48,512]{2,1,0:T(8,128)(2,1)S(1)} %bitcast.77), channel_id=1, replica_groups=mesh['sp'=8,'tp'=4] {'sp'}, dimensions={0} | all-to-all | bytes 786432 | tf_op jit(solution)/shard_map/all_to_all | solution.py:259
  31.8 15.1 %all_to_all.36 = bf16[8,48,512]{2,1,0:T(8,128)(2,1)} all-to-all(bf16[8,48,512]{2,1,0:T(8,128)(2,1)S(1)} %bitcast.80), channel_id=1, replica_groups=mesh['sp'=8,'tp'=4] {'sp'}, dimensions={0} | all-to-all | bytes 786432 | tf_op jit(solution)/shard_map/all_to_all | solution.py:259
  47.7 7.4 %shard_map.197 = (bf16[512,128]{1,0:T(8,128)(2,1)}, f32[256,128]{1,0:T(8,128)}, f32[128,128]{1,0:T(8,128)}, bf16[128,128]{1,0:T(8,128)(2,1)}, bf16[128,128]{1,0:T(8,128)(2,1)}) custom-call(bf16[128,128]{1,0:T(8,128)(2,1)} %q_ref.7, bf16[128,128]{1,0:T(8,128)(2,1)} %k_ref.5, bf16[256,128]{1,0:T(8,128)(2,1)} %v_ref.5, bf16[128,128]{1,0:T(8,128)(2,1)} %pre_ref.3, ...), custom_call_target="tpu_custom_call" | custom-call | flops 1073741824 | bytes 1048576 | tf_op jit(solution)/shard_map/pallas_call | solution.py:196
  55.1 2.6 %fusion.10 = f32[384,512]{1,0:T(8,128)S(1)} fusion(bf16[384,2048]{1,0:T(8,128)(2,1)} %all-gather.5.cloned.1.call-done, bf16[1,2048,512]{2,1,0:T(8,128)(2,1)S(1)} %copy-done), kind=kOutput, calls=%fused_computation.14 | convolution fusion | flops 805306368 | bytes 4456448 | tf_op jit(solution)/shard_map/dot_general | solution.py:276
  58.0 1.9 %fusion.6 = f32[384,512]{1,0:T(8,128)} fusion(bf16[384,2048]{1,0:T(8,128)(2,1)S(1)} %copy-done.11, bf16[1,2048,512]{2,1,0:T(8,128)(2,1)S(1)} %copy-done.1), kind=kOutput, calls=%fused_computation.10 | convolution fusion | flops 805306368 | bytes 4456448 | tf_op jit(solution)/shard_map/dot_general | solution.py:277
  59.8 9.5 %all-gather.3.cloned.1.call-done = bf16[384,2048]{1,0:T(8,128)(2,1)} async-done(((bf16[384,512]{1,0:T(8,128)(2,1)}), bf16[384,2048]{1,0:T(8,128)(2,1)}) %all-gather.3.cloned.1.call-update) | async-done | bytes 1572880 | tf_op jit(solution)/shard_map/all_gather | solution.py:260
  69.3 3.4 %multiply_convert_fusion.1 = (bf16[384,512]{1,0:T(8,128)(2,1)S(1)}, bf16[384,512]{1,0:T(8,128)(2,1)S(1)}) fusion(f32[384,512]{1,0:T(8,128)S(1)} %fusion.10, f32[384,512]{1,0:T(8,128)} %fusion.6, bf16[384,2048]{1,0:T(8,128)(2,1)} %all-gather.3.cloned.1.call-done, bf16[1,512,2048]{2,1,0:T(8,128)(2,1)} %param.27), kind=kOutput, calls=%fused_computation.23 | convolution fusion | flops 807862272 | bytes 6029312 | tf_op jit(solution)/shard_map/dot_general | solution.py:294
  74.7 2.2 %add_convert_fusion = bf16[384,2048]{1,0:T(8,128)(2,1)} fusion(f32[384,2048]{1,0:T(8,128)S(1)} %fusion.8, bf16[384,512]{1,0:T(8,128)(2,1)S(1)} %get-tuple-element.68, bf16[1,2048,512]{2,1,0:T(8,128)(2,1)S(1)} %copy-done.2), kind=kOutput, calls=%fused_computation | convolution fusion | flops 806879232 | bytes 7208960 | tf_op jit(solution)/shard_map/dot_general | solution.py:300
  77.0 14.9 %all_to_all.37.recv_ref.first_ref = bf16[8,128,128]{2,1,0:T(8,128)(2,1)} all-to-all(bf16[8,128,128]{2,1,0:T(8,128)(2,1)S(1)} %broadcast_select_fusion.1), channel_id=1, replica_groups=mesh['sp'=8,'tp'=4] {'sp'}, dimensions={0} | all-to-all | bytes 524288 | tf_op jit(solution)/shard_map/all_to_all | solution.py:280
  91.8 3.7 %shard_map.198 = (f32[128,128]{1,0:T(8,128)}, f32[256,128]{1,0:T(8,128)}, f32[32,128]{1,0:T(8,128)}, bf16[256,128]{1,0:T(8,128)(2,1)}) custom-call(s32[1]{0:T(128)} %bitcast.17.me_ref, bf16[8,128,128]{2,1,0:T(8,128)(2,1)} %all_to_all.37.recv_ref.first_ref, bf16[128,128]{1,0:T(8,128)(2,1)} %q_ref.7, f32[128,128]{1,0:T(8,128)} %get-tuple-element.44.cum_ref, ...), custom_call_target="tpu_custom_call" | custom-call | flops 268435456 | bytes 1048576 | tf_op jit(solution)/shard_map/pallas_call | solution.py:196
  96.5 17.9 %all_to_all.38 = bf16[8,256,128]{1,2,0:T(8,128)(2,1)S(1)} all-to-all(bf16[8,256,128]{1,2,0:T(8,128)(2,1)S(1)} %broadcast_in_dim.73), channel_id=1, replica_groups=mesh['sp'=8,'tp'=4] {'sp'}, dimensions={0} | all-to-all | bytes 1048576 | tf_op jit(solution)/shard_map/all_to_all | solution.py:287
  114.4 3.6 %all-to-all-start.4 = ((bf16[8,48,512]{2,1,0:T(8,128)(2,1)}), bf16[8,48,512]{2,1,0:T(8,128)(2,1)S(1)}, u32[]{:S(2)}, u32[]{:S(2)}) async-start(bf16[8,48,512]{2,1,0:T(8,128)(2,1)} %bitcast.78), calls=%async_computation.5 | async-start | bytes 786432 | tf_op jit(solution)/shard_map/all_to_all | solution.py:310
  118.0 11.4 %all-to-all-done.4 = bf16[8,48,512]{2,1,0:T(8,128)(2,1)S(1)} async-done(((bf16[8,48,512]{2,1,0:T(8,128)(2,1)}), bf16[8,48,512]{2,1,0:T(8,128)(2,1)S(1)}, u32[]{:S(2)}, u32[]{:S(2)}) %all-to-all-start.4) | async-done | bytes 393248 | tf_op jit(solution)/shard_map/all_to_all | solution.py:310
  129.7 6.5 %all_gather.11 = bf16[128,2048]{1,0:T(8,128)(2,1)S(1)} all-gather(bf16[128,512]{1,0:T(8,128)(2,1)S(1)} %fusion.12), channel_id=1, replica_groups=mesh['sp'=8,'tp'=4] {'tp'}, dimensions={1}, use_global_device_ids=true | all-gather | bytes 655360 | tf_op jit(solution)/shard_map/all_gather | solution.py:313
  136.2 2.4 %convolution_bitcast_fusion.1.gn_ref = f32[256,128]{1,0:T(8,128)} fusion(bf16[128,2048]{1,0:T(8,128)(2,1)S(1)} %all_gather.11, bf16[2048,256]{1,0:T(8,128)(2,1)} %param.20), kind=kOutput, calls=%fused_computation.21 | convolution fusion | flops 134217728 | bytes 1703936 | tf_op jit(solution)/shard_map/dot_general | solution.py:314
  138.6 3.2 %shard_map.199 = (f32[256,128]{1,0:T(8,128)}, bf16[128,128]{1,0:T(8,128)(2,1)}, bf16[128,128]{1,0:T(8,128)(2,1)}) custom-call(f32[256,128]{1,0:T(8,128)} %convolution_bitcast_fusion.1.gn_ref, f32[256,128]{1,0:T(8,128)} %get-tuple-element.48.normed_ref, f32[32,128]{1,0:T(8,128)} %get-tuple-element.49.inv_ref, bf16[128,128]{1,0:T(8,128)(2,1)} %q_ref.7, ...), custom_call_target="tpu_custom_call" | custom-call | flops 268435456 | bytes 1048576 | tf_op jit(solution)/shard_map/pallas_call | solution.py:196
  141.8 1.6 broadcast_select_fusion
  143.3 3.7 %all-to-all-start.5 = ((bf16[8,128,128]{2,1,0:T(8,128)(2,1)}), bf16[8,128,128]{2,1,0:T(8,128)(2,1)S(1)}, u32[]{:S(2)}, u32[]{:S(2)}) async-start(bf16[8,128,128]{2,1,0:T(8,128)(2,1)} %broadcast_select_fusion), calls=%async_computation.6 | async-start | bytes 524288 | tf_op jit(solution)/shard_map/all_to_all | solution.py:320
  147.0 8.5 %shard_map.200 = (f32[128,128]{1,0:T(8,128)}, f32[128,128]{1,0:T(8,128)}, f32[256,128]{1,0:T(8,128)}, f32[128,128]{1,0:T(8,128)}, f32[128,128]{1,0:T(8,128)}) custom-call(f32[256,128]{1,0:T(8,128)} %get-tuple-element.50.dm_ref, bf16[128,128]{1,0:T(8,128)(2,1)} %q_ref.7, bf16[128,128]{1,0:T(8,128)(2,1)} %k_ref.5, bf16[256,128]{1,0:T(8,128)(2,1)} %v_ref.5, ...), custom_call_target="tpu_custom_call" | custom-call | flops 2147483648 | bytes 1048576 | tf_op jit(solution)/shard_map/pallas_call | solution.py:196
  156.5 6.0 %all-to-all-start.6 = ((bf16[8,128,256]{1,2,0:T(8,128)(2,1)}), bf16[8,128,256]{1,2,0:T(8,128)(2,1)S(1)}, u32[]{:S(2)}, u32[]{:S(2)}) async-start(bf16[8,128,256]{1,2,0:T(8,128)(2,1)} %bitcast.74), calls=%async_computation.7 | async-start | bytes 1048576 | tf_op jit(solution)/shard_map/all_to_all | solution.py:330
  162.6 4.2 %fusion = bf16[1,2048,512]{2,1,0:T(8,128)(2,1)} fusion(bf16[384,2048]{1,0:T(8,128)(2,1)} %all-gather.5.cloned.1.call-done, bf16[384,512]{1,0:T(8,128)(2,1)} %copy-done.6), kind=kOutput, calls=%fused_computation.4 | convolution fusion | flops 806354944 | bytes 4063232 | tf_op jit(solution)/shard_map/dot_general | solution.py:307
  166.8 2.6 %fusion.1 = bf16[1,2048,512]{2,1,0:T(8,128)(2,1)} fusion(bf16[384,2048]{1,0:T(8,128)(2,1)S(1)} %copy-done.12, bf16[384,512]{1,0:T(8,128)(2,1)S(1)} %copy-done.5), kind=kOutput, calls=%fused_computation.5 | convolution fusion | flops 806354944 | bytes 4063232 | tf_op jit(solution)/shard_map/dot_general | solution.py:308
  169.4 2.7 %fusion.2 = bf16[1,512,2048]{2,1,0:T(8,128)(2,1)} fusion(bf16[384,2048]{1,0:T(8,128)(2,1)S(1)} %copy-done.13, f32[384,512]{1,0:T(8,128)S(1)} %copy-done.16, f32[384,512]{1,0:T(8,128)S(1)} %copy-done.15), kind=kOutput, calls=%fused_computation.6 | convolution fusion | flops 807534592 | bytes 5242880 | tf_op jit(solution)/shard_map/dot_general | solution.py:306
  172.1 4.1 %shard_map.201 = (f32[128,128]{1,0:T(8,128)}, f32[256,128]{1,0:T(8,128)}, f32[128,128]{1,0:T(8,128)}) custom-call(s32[1]{0:T(128)} %bitcast.17.me_ref, bf16[8,128,128]{2,1,0:T(8,128)(2,1)} %copy-done.3, bf16[8,128,128]{2,1,0:T(8,128)(2,1)} %all_to_all.37.recv_ref.first_ref, f32[128,128]{1,0:T(8,128)} %get-tuple-element.52.carried_ref, ...), custom_call_target="tpu_custom_call" | custom-call | flops 268435456 | bytes 1048576 | tf_op jit(solution)/shard_map/pallas_call | solution.py:196
  (62 shorter events, 12.4 us)
Async XLA Ops:
  7.2 47.9 %copy-start = (bf16[1,2048,512]{2,1,0:T(8,128)(2,1)S(1)}, bf16[1,2048,512]{2,1,0:T(8,128)(2,1)}, u32[]{:S(2)}) copy-start(bf16[1,2048,512]{2,1,0:T(8,128)(2,1)} %param.25) | copy-start | bytes 6291460
  7.2 47.9 %all-gather.5.cloned.1.call-start = ((), (), s32[]{:S(2)}) async-start(), calls=%async_computation.9 | async-start | bytes 1966080 | tf_op jit(solution)/shard_map/all_gather | solution.py:260
  10.3 36.7 %copy-start.10 = (f32[128]{0:T(128)S(1)}, f32[128]{0:T(128)}, u32[]{:S(2)}) copy-start(f32[128]{0:T(128)} %param.19) | copy-start | bytes 1540
  29.5 39.8 %all-gather.3.cloned.1.call-start = ((), (), s32[]{:S(2)}) async-start(), calls=%async_computation.8 | async-start | bytes 1966080 | tf_op jit(solution)/shard_map/all_gather | solution.py:260
  46.9 67.5 %reduce-scatter.2.cloned.1.call-start = ((), (), s32[]{:S(2)}) async-start(), calls=%async_computation.10 | async-start | bytes 1966080 | tf_op jit(solution)/shard_map/reduce_scatter | solution.py:303
  55.1 2.6 %copy-start.1 = (bf16[1,2048,512]{2,1,0:T(8,128)(2,1)S(1)}, bf16[1,2048,512]{2,1,0:T(8,128)(2,1)}, u32[]{:S(2)}) copy-start(bf16[1,2048,512]{2,1,0:T(8,128)(2,1)} %param.26) | copy-start | bytes 6291460
  55.1 2.9 %copy-start.11 = (bf16[384,2048]{1,0:T(8,128)(2,1)S(1)}, bf16[384,2048]{1,0:T(8,128)(2,1)}, u32[]{:S(2)}) copy-start(bf16[384,2048]{1,0:T(8,128)(2,1)} %all-gather.5.cloned.1.call-done) | copy-start | bytes 4718596
  58.0 11.3 %copy-start.14 = (f32[384,512]{1,0:T(8,128)}, f32[384,512]{1,0:T(8,128)S(1)}, u32[]{:S(2)}) copy-start(f32[384,512]{1,0:T(8,128)S(1)} %fusion.10) | copy-start | bytes 2359300
  72.8 1.0 copy-start.6
  72.8 1.0 copy-start.4
  72.8 1.9 %copy-start.2 = (bf16[1,2048,512]{2,1,0:T(8,128)(2,1)S(1)}, bf16[1,2048,512]{2,1,0:T(8,128)(2,1)}, u32[]{:S(2)}) copy-start(bf16[1,2048,512]{2,1,0:T(8,128)(2,1)} %param.26) | copy-start | bytes 6291460
  74.7 2.2 %copy-start.8 = (bf16[128,128]{1,0:T(8,128)(2,1)S(1)}, bf16[128,128]{1,0:T(8,128)(2,1)}, u32[]{:S(2)}) copy-start(bf16[128,128]{1,0:T(8,128)(2,1)} %get-tuple-element.42) | copy-start | bytes 98308
  74.7 2.2 %copy-start.9 = (bf16[128,128]{1,0:T(8,128)(2,1)S(1)}, bf16[128,128]{1,0:T(8,128)(2,1)}, u32[]{:S(2)}) copy-start(bf16[128,128]{1,0:T(8,128)(2,1)} %get-tuple-element.43) | copy-start | bytes 98308
  77.0 52.4 %copy-start.7 = (bf16[128,512]{1,0:T(8,128)(2,1)S(1)}, bf16[128,512]{1,0:T(8,128)(2,1)}, u32[]{:S(2)}) copy-start(bf16[128,512]{1,0:T(8,128)(2,1)} %param.24) | copy-start | bytes 393220
  114.4 15.0 %all-to-all-start.4 = ((bf16[8,48,512]{2,1,0:T(8,128)(2,1)}), bf16[8,48,512]{2,1,0:T(8,128)(2,1)S(1)}, u32[]{:S(2)}, u32[]{:S(2)}) async-start(bf16[8,48,512]{2,1,0:T(8,128)(2,1)} %bitcast.78), calls=%async_computation.5 | async-start | bytes 786432 | tf_op jit(solution)/shard_map/all_to_all | solution.py:310
  143.3 13.2 %all-to-all-start.5 = ((bf16[8,128,128]{2,1,0:T(8,128)(2,1)}), bf16[8,128,128]{2,1,0:T(8,128)(2,1)S(1)}, u32[]{:S(2)}, u32[]{:S(2)}) async-start(bf16[8,128,128]{2,1,0:T(8,128)(2,1)} %broadcast_select_fusion), calls=%async_computation.6 | async-start | bytes 524288 | tf_op jit(solution)/shard_map/all_to_all | solution.py:320
  156.5 10.2 %copy-start.3 = (bf16[8,128,128]{2,1,0:T(8,128)(2,1)}, bf16[8,128,128]{2,1,0:T(8,128)(2,1)S(1)}, u32[]{:S(2)}) copy-start(bf16[8,128,128]{2,1,0:T(8,128)(2,1)S(1)} %all-to-all-done.5.recv_ref) | copy-start | bytes 786436
  156.5 20.4 %all-to-all-start.6 = ((bf16[8,128,256]{1,2,0:T(8,128)(2,1)}), bf16[8,128,256]{1,2,0:T(8,128)(2,1)S(1)}, u32[]{:S(2)}, u32[]{:S(2)}) async-start(bf16[8,128,256]{1,2,0:T(8,128)(2,1)} %bitcast.74), calls=%async_computation.7 | async-start | bytes 1048576 | tf_op jit(solution)/shard_map/all_to_all | solution.py:330
  162.5 4.2 %copy-start.5 = (bf16[384,512]{1,0:T(8,128)(2,1)S(1)}, bf16[384,512]{1,0:T(8,128)(2,1)}, u32[]{:S(2)}) copy-start(bf16[384,512]{1,0:T(8,128)(2,1)} %copy-done.4) | copy-start | bytes 1179652
  162.6 4.2 %copy-start.12 = (bf16[384,2048]{1,0:T(8,128)(2,1)S(1)}, bf16[384,2048]{1,0:T(8,128)(2,1)}, u32[]{:S(2)}) copy-start(bf16[384,2048]{1,0:T(8,128)(2,1)} %all-gather.5.cloned.1.call-done) | copy-start | bytes 4718596
  166.8 2.6 %copy-start.13 = (bf16[384,2048]{1,0:T(8,128)(2,1)S(1)}, bf16[384,2048]{1,0:T(8,128)(2,1)}, u32[]{:S(2)}) copy-start(bf16[384,2048]{1,0:T(8,128)(2,1)} %all-gather.3.cloned.1.call-done) | copy-start | bytes 4718596
  166.8 2.6 %copy-start.15 = (f32[384,512]{1,0:T(8,128)S(1)}, f32[384,512]{1,0:T(8,128)}, u32[]{:S(2)}) copy-start(f32[384,512]{1,0:T(8,128)} %copy-done.14) | copy-start | bytes 2359300
  166.8 2.6 %copy-start.16 = (f32[384,512]{1,0:T(8,128)S(1)}, f32[384,512]{1,0:T(8,128)}, u32[]{:S(2)}) copy-start(f32[384,512]{1,0:T(8,128)} %fusion.6) | copy-start | bytes 2359300
Sparse Core Ops, SparseCore 0:
  29.7 18.3 all-gather.4
  49.6 19.6 all-gather.2
  77.0 27.9 reduce-scatter.1
where the time goes:
time: 186 us; the launch traced here: 185 us
  blocking collectives  73.6 us (40%)
  Pallas kernels  26.9 us (14%)
  matrix products  25.9 us (14%)
  waiting for transfers between devices  21.7 us (12%)
  between operations  14 us (8%)
  starting transfers between devices  13.4 us (7%)
  local copies, waits for them, and re-layouts  5.48 us (3%)
  other arithmetic  3.55 us (2%)
    all_to_all x2, blocking collectives, exchange(): rows = lax.all_to_all(rows, 'sp', split_axis=0, concat_axis=0, tiled=True)  34.3 us
    pallas_call x5, Pallas kernels, per_head(): pl.pallas_call(kernel, grid=(heads,), in_specs=in_specs, out_specs=[spec(...  26.9 us
    all_to_all x1, blocking collectives, body(): lax.all_to_all(jnp.broadcast_to(mix_rows[None], (experts, values, tok_row...  17.9 us
    all_to_all x1, blocking collectives, body(): lax.all_to_all(jnp.where(peer > index, fwd_sum[None], bwd_sum[None]), 'sp...  14.9 us
    all_to_all x1, waiting for transfers between devices, body(): lax.all_to_all(summed, 'sp', split_axis=0, concat_axis=0, tiled=True)  11.4 us
    all_gather x2, waiting for transfers between devices, exchange(): lax.all_gather(rows.reshape(slots, part_width), 'tp', axis=1, tiled=True)  9.48 us
    all_gather x1, blocking collectives, body(): full_rows = lax.all_gather(grad_rows, 'tp', axis=1, tiled=True)  6.5 us
    all_to_all x1, starting transfers between devices, body(): lax.all_to_all(full_rows.reshape(tok_rows, experts, rows_block).swapaxes(...  6 us
  transfers between devices with their start and end apart: 6, of which 3 were waited for; matrix products, arithmetic and copies ran while one was open for 10% of the time, Pallas kernels for 13%

commit v1 on v0

--- a/solution.py
+++ b/solution.py
@@ -9,8 +9,14 @@
 
 KEY_DIM = 32
 VAL_DIM = 64
+CORES = 2
 BF16 = jnp.bfloat16
 F32 = jnp.float32
+MESH = pl.DeviceIdType.MESH
+VMEM_LIMIT = 60 * 1024 * 1024
+TN = ((0,), (0,))
+NN = ((1,), (0,))
+NT = ((1,), (1,))
 
 
 def dot(a, b, contract):
@@ -29,77 +35,326 @@
     return test(rows, cols)
 
 
-def head_kernel(q_ref, k_ref, v_ref, pre_ref, extra_ref, speed_ref,
-                st_ref, inner_ref, cum_ref, fwd_ref, bwd_ref):
-    length = q_ref.shape[1]
-    q = q_ref[...].astype(F32) * KEY_DIM ** (-0.5)
-    k = k_ref[...].astype(F32)
-    v = v_ref[...]
+def loop(count, step):
+    lax.fori_loop(0, count, lambda i, _: (step(i), 0)[1], 0)
+
+
+class Peers:
+    def __init__(self, n, m):
+        self.n, self.m, self.chips = n, m, m // CORES
+        self.me, self.tp = lax.axis_index("sp"), lax.axis_index("tp")
+        self.chip, self.core = lax.div(self.tp, CORES), lax.rem(self.tp, CORES)
+        self.mate = self.chip * CORES + (1 - self.core)
+
+    def to(self, d):
+        return lax.rem(self.me + d, self.n)
+
+    def source(self, d):
+        return lax.rem(self.me - d + self.n, self.n)
+
+    def to_chip(self, d):
+        return lax.rem(self.chip + d, self.chips) * CORES + self.core
+
+    def from_chip(self, d):
+        return lax.rem(self.chip - d + self.chips, self.chips) * CORES + self.core
+
+    def mate_from_chip(self, d):
+        return lax.rem(self.chip - d + self.chips, self.chips) * CORES + (1 - self.core)
+
+    def greet(self):
+        barrier = pltpu.get_barrier_semaphore()
+
+        def signal(device):
+            pl.semaphore_signal(barrier, inc=1, device_id=device, device_id_type=MESH)
+
+        loop(self.n - 1, lambda i: signal({"sp": self.to(i + 1)}))
+        for d in range(1, self.chips):
+            signal({"tp": self.to_chip(d)})
+        signal({"tp": self.mate})
+
+    def met(self):
+        pl.semaphore_wait(pltpu.get_barrier_semaphore(), self.n - 1 + self.chips)
+
+
+def copy_to(src, dst, send, recv, device):
+    return pltpu.make_async_remote_copy(src_ref=src, dst_ref=dst, send_sem=send, recv_sem=recv,
+                                        device_id=device, device_id_type=MESH)
+
+
+def own_heads(stacked, width):
+    heads = stacked.shape[0] // width
+    head = lax.broadcasted_iota(jnp.int32, (width, stacked.shape[1]), 1) // KEY_DIM
+    out = jnp.zeros((width, stacked.shape[1]), F32)
+    for h in range(heads):
+        out = jnp.where(head == h, stacked[h * width:(h + 1) * width], out)
+    return out
+
+
+def spread_heads(state, heads):
+    head = lax.broadcasted_iota(jnp.int32, state.shape, 1) // KEY_DIM
+    return jnp.concatenate([jnp.where(head == h, state, 0.0) for h in range(heads)], axis=0)
+
+
+def as_row(column):
+    length = column.shape[0]
+    diagonal = triangle(length, lambda a, b: a == b)
+    return jnp.sum(jnp.where(diagonal, column, 0.0), axis=0, keepdims=True)
+
+
+def as_column(row):
+    length = row.shape[1]
+    diagonal = triangle(length, lambda a, b: a == b)
+    return jnp.sum(jnp.where(diagonal, row, 0.0), axis=1, keepdims=True)
+
+
+def carry(n, me, state_of, factor_of):
+    shape = state_of(0).shape
+    before, after = jnp.zeros(shape, F32), jnp.zeros(shape, F32)
+    for i in range(n):
+        before = jnp.where(i < me, before * factor_of(i) + state_of(i), before)
+    for i in reversed(range(n)):
+        after = jnp.where(i > me, after * factor_of(i) + state_of(i), after)
+    return before, after
+
+
+def dispatch_kernel(n, m, cap, q_ref, k_ref, v_ref, pre_ref, extra_ref, speed_ref, x_ref, cot_ref,
+                    pick_ref, comb_ref, gate_any, up_any, down_any,
+                    rows_ref, hidden_ref, ggp_ref, gup_ref, place_ref, st_ref, cum_ref,
+                    normed_ref, inv_ref, mix_ref, carried_ref, last_ref,
+                    send_ref, sbuf, sin, lbuf, inner_ref, gate_v, up_v, down_v, gp_ref, up_ref,
+                    zs, zr, ys, yr, ps, pr, ss, sr, ws):
+    at = Peers(n, m)
+    me = at.me
+    tok, channels = q_ref.shape[1], q_ref.shape[0]
+    width = x_ref.shape[1]
+    heads = channels // KEY_DIM
+    slots = n * cap
+    at.greet()
+    loads = [pltpu.make_async_copy(src, dst, ws.at[i])
+             for i, (src, dst) in enumerate(((gate_any, gate_v), (up_any, up_v),
+                                             (down_any, down_v)))]
+    for load in loads:
+        load.start()
+
+    expert = lax.broadcasted_iota(jnp.int32, (n, tok), 0)
+    picks = [pick_ref[i:i + 1, :] == expert for i in range(2)]
+    named = (picks[0] | picks[1]).astype(F32)
+    counts = dot(named, triangle(tok, lambda a, b: a < b).astype(F32), NN)
+    slot = lax.broadcasted_iota(jnp.int32, (slots, tok), 0)
+    places = []
+    for i in range(2):
+        rank = jnp.sum(jnp.where(picks[i], counts, 0.0), axis=0, keepdims=True)
+        places.append(slot == pick_ref[i:i + 1, :] * cap + rank.astype(jnp.int32))
+    place = (places[0] | places[1]).astype(BF16)
+    place_ref[...] = place
+    weight = jnp.sum(jnp.where(places[0], comb_ref[0:1, :], 0.0)
+                     + jnp.where(places[1], comb_ref[1:2, :], 0.0), axis=1, keepdims=True)
+    send_ref[0] = dot(place, x_ref[...], NN).astype(BF16)
+    send_ref[1] = (weight * dot(place, cot_ref[...], NN)).astype(BF16)
+
+    def rows(p):
+        return pl.ds(pl.multiple_of(p * cap, 16), cap)
+
+    for t in range(2):
+        rows_ref[t, at.tp, rows(me), :] = send_ref[t, rows(me), :]
+
+    def out_row(t, d):
+        p = at.to(d)
+        return copy_to(send_ref.at[t, rows(p)], rows_ref.at[t, at.tp, rows(me)],
+                       zs.at[t, d], zr.at[t, d], {"sp": p})
+
+    def in_row(t, d):
+        p = at.source(d)
+        here = rows_ref.at[t, at.tp, rows(p)]
+        return copy_to(here, here, zs.at[t, d], zr.at[t, d], {"sp": p})
+
+    def across(t, d, dy):
+        here = rows_ref.at[t, at.tp, rows(at.source(d))]
+        return copy_to(here, here, ys.at[t, dy, d], yr.at[t, dy, d], {"tp": at.to_chip(dy)})
+
+    def across_in(t, d, dy):
+        here = rows_ref.at[t, at.from_chip(dy), rows(at.source(d))]
+        return copy_to(here, here, ys.at[t, dy, d], yr.at[t, dy, d], {"tp": at.from_chip(dy)})
+
+    def relay(t, d, dy):
+        here = rows_ref.at[t, at.from_chip(dy), rows(at.source(d))]
+        return copy_to(here, here, ps.at[t, dy, d], pr.at[t, dy, d], {"tp": at.mate})
+
+    def relay_in(t, d, dy):
+        here = rows_ref.at[t, at.mate_from_chip(dy), rows(at.source(d))]
+        return copy_to(here, here, ps.at[t, dy, d], pr.at[t, dy, d], {"tp": at.mate})
+
+    def pass_on(t, d):
+        @pl.when(d > 0)
+        def _():
+            in_row(t, d).wait_recv()
+        for dy in range(1, at.chips):
+            across(t, d, dy).start()
+        relay(t, d, 0).start()
+
+    def pass_mate(t, d):
+        for dy in range(1, at.chips):
+            across_in(t, d, dy).wait_recv()
+            relay(t, d, dy).start()
+
+    def gathered(t, d):
+        for dy in range(at.chips):
+            relay_in(t, d, dy).wait_recv()
+
+    at.met()
+    for t in range(2):
+        loop(n - 1, lambda i, t=t: out_row(t, i + 1).start())
+
     pre = pre_ref[...].astype(F32)
     log_sig = jnp.minimum(pre, 0.0) - jnp.log1p(jnp.exp(-jnp.abs(pre)))
-    decays = speed_ref[...] * log_sig + extra_ref[...]
-    upto = triangle(length, lambda a, b: a <= b).astype(F32)
-    cum = exact_dot(decays, upto)
-    cum_ref[...] = cum
-    cum_t = cum.T
-    k_t = k.T
-    total = jnp.zeros((length, length), F32)
-    for c in range(KEY_DIM):
-        weight = jnp.exp(-jnp.abs(cum_t[:, c:c + 1] - cum[c:c + 1, :]))
-        total = total + (k_t[:, c:c + 1] * q[c:c + 1, :]) * weight
-    scores = total.astype(BF16)
-    st_ref[...] = scores
-    inner_ref[...] = dot(v, scores, ((1,), (0,)))
-    last = cum[:, length - 1:length]
-    fwd = dot(k * jnp.exp(last - cum), v, ((1,), (1,)))
-    bwd = dot(k * jnp.exp(cum), v, ((1,), (1,)))
-    high = last.astype(BF16)
-    rest = last - high.astype(F32)
-    middle = rest.astype(BF16)
-    low = (rest - middle.astype(F32)).astype(BF16)
-    lane = lax.broadcasted_iota(jnp.int32, (KEY_DIM, VAL_DIM), 1)
-    logs = jnp.where(lane == 0, high.astype(F32),
-                     jnp.where(lane == 1, middle.astype(F32), low.astype(F32)))
-    fwd_ref[...] = jnp.concatenate([fwd, logs], axis=1).astype(BF16)
-    bwd_ref[...] = jnp.concatenate([bwd, logs], axis=1).astype(BF16)
-
-
-def carry(recv, me, sums_of, factors):
-    peers = recv.shape[0]
-    zero = jnp.zeros((KEY_DIM, VAL_DIM), F32)
-    before, after = zero, zero
-    for i in range(peers):
-        before = jnp.where(i < me, before * factors[i] + sums_of(i), before)
-    for i in reversed(range(peers)):
-        after = jnp.where(i > me, after * factors[i] + sums_of(i), after)
-    return before, after
-
-
-def factors_of(recv):
-    out = []
-    for i in range(recv.shape[0]):
-        logs = recv[i, :, VAL_DIM:VAL_DIM + 3].astype(F32)
-        out.append(jnp.exp(logs[:, 0:1] + logs[:, 1:2] + logs[:, 2:3]))
-    return out
-
-
-def mix_kernel(me_ref, recv_ref, q_ref, cum_ref, inner_ref,
-               carried_ref, normed_ref, inv_ref, rows_ref):
-    length = q_ref.shape[1]
-    me = me_ref[0]
-    fwd_in, bwd_in = carry(
-        recv_ref, me, lambda i: recv_ref[i, :, :VAL_DIM].astype(F32), factors_of(recv_ref))
-    carried_ref[...] = jnp.concatenate([fwd_in, bwd_in], axis=1)
+    decays = as_column(speed_ref[...]) * log_sig + extra_ref[...]
+    cum_ref[...] = exact_dot(decays, triangle(tok, lambda a, b: a <= b).astype(F32))
+
+    per_head = -(-n // heads)
+
+    def head(h):
+        keys = pl.ds(pl.multiple_of(h * KEY_DIM, KEY_DIM), KEY_DIM)
+        values = pl.ds(pl.multiple_of(h * VAL_DIM, VAL_DIM), VAL_DIM)
+        q = q_ref[keys, :].astype(F32) * KEY_DIM ** (-0.5)
+        cum = cum_ref[keys, :]
+        cum_t = cum.T
+        k_t = k_ref[keys, :].astype(F32).T
+        total = jnp.zeros((tok, tok), F32)
+        for c in range(KEY_DIM):
+            decay = jnp.exp(-jnp.abs(cum_t[:, c:c + 1] - cum[c:c + 1, :]))
+            total = total + (k_t[:, c:c + 1] * q[c:c + 1, :]) * decay
+        scores = total.astype(BF16)
+        st_ref[pl.ds(pl.multiple_of(h * tok, tok), tok), :] = scores
+        inner_ref[values, :] = dot(v_ref[values, :], scores, NN)
+
+        def forward(i):
+            @pl.when(h * per_head + i < n)
+            def _():
+                pass_on(0, h * per_head + i)
+        loop(per_head, forward)
+
+    loop(heads, head)
+
+    cum = cum_ref[...]
+    last = cum[:, tok - 1:tok]
+    k = k_ref[...].astype(F32)
+    sbuf[0] = own_heads(dot(v_ref[...], k * jnp.exp(last - cum), NT), VAL_DIM).astype(BF16)
+    sbuf[1] = own_heads(dot(v_ref[...], k * jnp.exp(cum), NT), VAL_DIM).astype(BF16)
+    lbuf[...] = jnp.broadcast_to(as_row(last), lbuf.shape)
+    sin[me] = jnp.zeros(sin.shape[1:], BF16)
+    last_ref[me] = jnp.zeros(last_ref.shape[1:], F32)
+
+    def out_state(d):
+        p = at.to(d)
+        return (copy_to(sbuf.at[jnp.where(p > me, 0, 1)], sin.at[me], ss.at[0, d], sr.at[0, d],
+                        {"sp": p}),
+                copy_to(lbuf, last_ref.at[me], ss.at[1, d], sr.at[1, d], {"sp": p}))
+
+    def in_state(d):
+        p = at.source(d)
+        return (copy_to(sbuf.at[0], sin.at[p], ss.at[0, d], sr.at[0, d], {"sp": p}),
+                copy_to(lbuf, last_ref.at[p], ss.at[1, d], sr.at[1, d], {"sp": p}))
+
+    loop(n - 1, lambda i: [copy.start() for copy in out_state(i + 1)] and None)
+
+    half = n // 2
+    loop(n, lambda d: pass_mate(0, d))
+    loop(half, lambda d: pass_on(1, d))
+    loop(n, lambda d: gathered(0, d))
+
+    def columns_of(weights, t):
+        total = None
+        for j in range(m):
+            part = dot(rows_ref[t, j], weights[j * width:(j + 1) * width, :], NN)
+            total = part if total is None else total + part
+        return total
+
+    loads[0].wait()
+    gp_ref[...] = columns_of(gate_v, 0)
+    loop(n - half, lambda d: pass_on(1, d + half))
+    loads[1].wait()
+    up_ref[...] = columns_of(up_v, 0)
+    loop(n, lambda d: pass_mate(1, d))
+
+    loop(n - 1, lambda i: [copy.wait_recv() for copy in in_state(i + 1)] and None)
+    before, after = carry(n, me, lambda i: sin[i].astype(F32),
+                          lambda i: jnp.exp(last_ref[i, 0:1, :]))
+    carried_ref[0] = before
+    carried_ref[1] = after
     q = q_ref[...].astype(F32) * KEY_DIM ** (-0.5)
-    cum = cum_ref[...]
-    last = cum[:, length - 1:length]
-    mixed = inner_ref[...] + dot(fwd_in, q * jnp.exp(cum), ((0,), (0,)))
-    mixed = mixed + dot(bwd_in, q * jnp.exp(last - cum), ((0,), (0,)))
-    inv = lax.rsqrt(jnp.mean(mixed * mixed, axis=0, keepdims=True) + 1e-06)
-    normed = mixed * inv
-    normed_ref[...] = normed
-    inv_ref[...] = jnp.broadcast_to(inv, inv_ref.shape)
-    rows_ref[...] = normed.astype(BF16)
+    mixed = inner_ref[...] + dot(spread_heads(before, heads), q * jnp.exp(cum), NN)
+    mixed = mixed + dot(spread_heads(after, heads), q * jnp.exp(last - cum), NN)
+    for h in range(heads):
+        part = mixed[h * VAL_DIM:(h + 1) * VAL_DIM]
+        inv = lax.rsqrt(jnp.mean(part * part, axis=0, keepdims=True) + 1e-06)
+        normed = part * inv
+        normed_ref[h * VAL_DIM:(h + 1) * VAL_DIM, :] = normed
+        mix_ref[h * VAL_DIM:(h + 1) * VAL_DIM, :] = normed.astype(BF16)
+        inv_ref[h * 8:(h + 1) * 8, :] = jnp.broadcast_to(inv, (8, tok))
+
+    loop(n, lambda d: gathered(1, d))
+    loads[2].wait()
+    grad_hidden = None
+    for j in range(m):
+        part = dot(rows_ref[1, j], down_v[:, j * width:(j + 1) * width], NT)
+        grad_hidden = part if grad_hidden is None else grad_hidden + part
+    gate_pre, up_pre = gp_ref[...], up_ref[...]
+    gate_sig = jax.nn.sigmoid(gate_pre)
+    gate_act = gate_pre * gate_sig
+    hidden_ref[...] = (gate_act * up_pre).astype(BF16)
+    ggp_ref[...] = (grad_hidden * up_pre * gate_sig
+                    * (1.0 + gate_pre * (1.0 - gate_sig))).astype(BF16)
+    gup_ref[...] = (grad_hidden * gate_act).astype(BF16)
+
+    def drain(i):
+        for copy in out_state(i + 1):
+            copy.wait_send()
+        for t in range(2):
+            out_row(t, i + 1).wait_send()
+    loop(n - 1, drain)
+
+    def drain_passed(d):
+        for t in range(2):
+            for dy in range(1, at.chips):
+                across(t, d, dy).wait_send()
+            for dy in range(at.chips):
+                relay(t, d, dy).wait_send()
+    loop(n, drain_passed)
+
+
+def vmem_specs(count):
+    return [pl.BlockSpec(memory_space=pltpu.VMEM)] * count
+
+
+def dispatch(n, m, cap, q, k, v, pre, extra, speed, x, cot, picks, comb, gate, up, down):
+    channels, tok = q.shape
+    values = v.shape[0]
+    heads = channels // KEY_DIM
+    slots, width, units = n * cap, x.shape[1], gate.shape[1]
+    chips = m // CORES
+    dma = pltpu.SemaphoreType.DMA
+    outs = [((2, m, slots, width), BF16), ((slots, units), BF16), ((slots, units), BF16),
+            ((slots, units), BF16), ((slots, tok), BF16), ((heads * tok, tok), BF16),
+            ((channels, tok), F32), ((values, tok), F32), ((heads * 8, tok), F32),
+            ((values, tok), BF16), ((2, VAL_DIM, channels), F32), ((n, 8, channels), F32)]
+    return pl.pallas_call(
+        functools.partial(dispatch_kernel, n, m, cap),
+        in_specs=vmem_specs(10) + [pl.BlockSpec(memory_space=pl.ANY)] * 3,
+        out_specs=vmem_specs(len(outs)),
+        out_shape=[jax.ShapeDtypeStruct(shape, dtype) for shape, dtype in outs],
+        scratch_shapes=[
+            pltpu.VMEM((2, slots, width), BF16), pltpu.VMEM((2, VAL_DIM, channels), BF16),
+            pltpu.VMEM((n, VAL_DIM, channels), BF16), pltpu.VMEM((8, channels), F32),
+            pltpu.VMEM((values, tok), F32),
+            pltpu.VMEM(gate.shape, BF16), pltpu.VMEM(up.shape, BF16), pltpu.VMEM(down.shape, BF16),
+            pltpu.VMEM((slots, units), F32), pltpu.VMEM((slots, units), F32),
+            dma((2, n)), dma((2, n)), dma((2, chips, n)), dma((2, chips, n)),
+            dma((2, chips, n)), dma((2, chips, n)), dma((2, n)), dma((2, n)), dma((3,)),
+        ],
+        compiler_params=pltpu.CompilerParams(collective_id=0, has_side_effects=True,
+                                             vmem_limit_bytes=VMEM_LIMIT),
+        name="dispatch",
+    )(q, k, v, pre, extra, speed, x, cot, picks, comb, gate, up, down)
 
 
 def source_kernel(gn_ref, normed_ref, inv_ref, q_ref, cum_ref, dm_ref, fwd_ref, bwd_ref):
@@ -162,7 +417,8 @@
     length = k_ref.shape[1]
     me = me_ref[0]
     grad_bwd, grad_fwd = carry(
-        recv_ref, me, lambda i: recv_ref[i, :, :VAL_DIM].astype(F32), factors_of(first_ref))
+        recv_ref.shape[0], me, lambda i: recv_ref[i, :, :VAL_DIM].astype(F32),
+        lambda i: jnp.exp(first_ref[i, :, 0:1]))
     k = k_ref[...].astype(F32)
     v = v_ref[...]
     cum = cum_ref[...]
@@ -223,10 +479,10 @@
 ):
     heads = input_value_matrix.shape[0] // VAL_DIM
     tok_rows = queries.shape[1]
-    experts = lax.axis_size("sp")
+    experts, m = lax.axis_size("sp"), lax.axis_size("tp")
     index = lax.axis_index("sp")
     me = index.astype(jnp.int32).reshape(1)
-    capacity = 3 * tok_rows // experts
+    capacity = -(-(3 * tok_rows // experts) // 16) * 16
     slots = experts * capacity
     part_width = stored_expert_rows.shape[1]
     model_width = expert_gate_weight.shape[1]
@@ -234,68 +490,22 @@
     values = heads * VAL_DIM
     tn = (((0,), (0,)), ((), ()))
     nt = (((1,), (1,)), ((), ()))
-
-    expert_ids = lax.broadcasted_iota(jnp.int32, (tok_rows, experts), 1)
-    picks = [chosen_expert_index[:, i:i + 1] == expert_ids for i in range(2)]
-    earlier = triangle(tok_rows, lambda a, b: a > b).astype(BF16)
-    counts = jnp.dot(earlier, (picks[0] | picks[1]).astype(BF16), preferred_element_type=F32)
-    slot_ids = lax.broadcasted_iota(jnp.int32, (tok_rows, slots), 1)
-    places = []
-    for i in range(2):
-        rank = jnp.sum(jnp.where(picks[i], counts, 0.0), axis=1, keepdims=True)
-        slot = chosen_expert_index[:, i:i + 1] * capacity + rank.astype(jnp.int32)
-        places.append((slot == slot_ids).astype(BF16))
-    place = places[0] + places[1]
-    weighted = [
-        (expert_combine_weight[:, i:i + 1] * cotangent.astype(F32)).astype(BF16)
-        for i in range(2)
-    ]
-    send_x = lax.dot_general(place, stored_expert_rows, tn, preferred_element_type=F32)
-    send_dy = lax.dot_general(jnp.concatenate(places, axis=0), jnp.concatenate(weighted, axis=0),
-                              tn, preferred_element_type=F32)
-
-    def exchange(rows):
-        rows = rows.astype(BF16).reshape(experts, capacity, part_width)
-        rows = lax.all_to_all(rows, "sp", split_axis=0, concat_axis=0, tiled=True)
-        return lax.all_gather(rows.reshape(slots, part_width), "tp", axis=1, tiled=True)
-
-    rows_x = exchange(send_x)
-    rows_dy = exchange(send_dy)
-
+    gate_local, up_local, down_local = expert_gate_weight[0], expert_up_weight[0], expert_down_weight[0]
+    (rows, hidden, grad_gate_pre, grad_up_pre, place, scores, cum, normed, inv_rms, mix_rows,
+     carried, lasts) = dispatch(
+        experts, m, capacity, queries, input_key_matrix, input_value_matrix,
+        decay_preactivation, extra_log_decay, channel_decay_speed[None, :], stored_expert_rows,
+        cotangent, chosen_expert_index.T, expert_combine_weight.T, gate_local, up_local, down_local)
+    rows_x = rows[0].swapaxes(0, 1).reshape(slots, m * part_width)
+    rows_dy = rows[1].swapaxes(0, 1).reshape(slots, m * part_width)
+    carried = jnp.concatenate([carried[0].T, carried[1].T], axis=1)
+    sums = lasts.swapaxes(1, 2)
+    place = place.T
     speed = channel_decay_speed[:, None]
     state = ((channels, 2 * VAL_DIM), BF16)
-    scores, inner, cum, fwd_sum, bwd_sum = per_head(
-        head_kernel, heads,
-        [((heads * tok_rows, tok_rows), BF16), ((values, tok_rows), F32),
-         ((channels, tok_rows), F32), state, state],
-        [queries, input_key_matrix, input_value_matrix, decay_preactivation, extra_log_decay,
-         speed], 1 << 28)
     peer = lax.broadcasted_iota(jnp.int32, (experts, 1, 1), 0)
-    gate_local = expert_gate_weight[0]
-    up_local = expert_up_weight[0]
-    gate_pre = jnp.dot(rows_x, gate_local, preferred_element_type=F32)
-    up_pre = jnp.dot(rows_x, up_local, preferred_element_type=F32)
-    rows_dy, fwd_sum, bwd_sum, gate_pre, up_pre = lax.optimization_barrier(
-        (rows_dy, fwd_sum, bwd_sum, gate_pre, up_pre))
-    sums = lax.all_to_all(jnp.where(peer > index, fwd_sum[None], bwd_sum[None]),
-                          "sp", split_axis=0, concat_axis=0, tiled=True)
-    carried, normed, inv_rms, mix_rows = per_head(
-        mix_kernel, heads,
-        [((channels, 2 * VAL_DIM), F32), ((values, tok_rows), F32), ((heads * 8, tok_rows), F32),
-         ((values, tok_rows), BF16)],
-        [me, sums, queries, cum, inner], 1 << 26, scalars=1)
     all_mix = lax.all_to_all(jnp.broadcast_to(mix_rows[None], (experts, values, tok_rows)),
                              "sp", split_axis=0, concat_axis=0, tiled=True)
-
-    down_local = expert_down_weight[0]
-    gate_sig = jax.nn.sigmoid(gate_pre)
-    gate_act = gate_pre * gate_sig
-    hidden = (gate_act * up_pre).astype(BF16)
-    grad_hidden = lax.dot_general(rows_dy, down_local, nt, preferred_element_type=F32)
-    grad_gate_pre = (grad_hidden * up_pre * gate_sig * (1.0 + gate_pre * (1.0 - gate_sig))).astype(
-        BF16
-    )
-    grad_up_pre = (grad_hidden * gate_act).astype(BF16)
     partial_value = lax.dot_general(grad_gate_pre, gate_local, nt, preferred_element_type=F32)
     partial_value = partial_value + lax.dot_general(
         grad_up_pre, up_local, nt, preferred_element_type=F32

time: 186 us -> 162 us (0.87)
  blocking collectives: 73.6 us -> 30.6 us
  Pallas kernels: 26.9 us -> 52 us
  matrix products: 25.9 us -> 17.2 us
  local copies, waits for them, and re-layouts: 5.48 us -> 9.91 us
  starting transfers between devices: 13.4 us -> 15.3 us
    all_to_all x3 -> x0, blocking collectives: 49.2 us -> none  [the longest x2 34.3 us: exchange(): rows = lax.all_to_all(rows, 'sp', split_axis=0, concat_axis=0, tiled=True)]
    pallas_call x0 -> x1, Pallas kernels: none -> 36.2 us  [dispatch(): pl.pallas_call(functools.partial(dispatch_kernel, n, m, cap), in_specs=vm...]
    pallas_call x5 -> x3, Pallas kernels: 26.9 us -> 15.7 us  [per_head(): pl.pallas_call(kernel, grid=(heads,), in_specs=in_specs, out_specs=[spec(...]
    dot_general x6 -> x0, matrix products: 9.6 us -> none  [the longest x1 3.43 us: body(): lax.dot_general(rows_dy, down_local, nt, preferred_element_type=F32)]
    all_gather x2 -> x0, waiting for transfers between devices: 9.48 us -> none  [exchange(): lax.all_gather(rows.reshape(slots, part_width), 'tp', axis=1, tiled=True)]
    reduce_scatter x1, waiting for transfers between devices: 0.01 us -> 8.61 us  [body(): lax.psum_scatter(partial_value.astype(BF16), 'tp', scatter_dimension=1, t...]
    transpose x0 -> x4, local copies, waits for them, and re-layouts: none -> 6.84 us  [the longest x2 5.27 us: body(): rows_dy = rows[1].swapaxes(0, 1).reshape(slots, m * part_width)]
    all_to_all x1, blocking collectives: 17.9 us -> 24.1 us  [body(): lax.all_to_all(jnp.broadcast_to(mix_rows[None], (experts, values, tok_row...]
  transfers between devices with their start and end apart: 6 -> 4, of which waited for: 3 -> 2; matrix products, arithmetic and copies ran while one was open for 10% -> 12% of each run, Pallas kernels for 13% -> 8%
where the time goes in v1:
time: 162 us; the launch traced here: 161 us
  Pallas kernels  52 us (32%)
  blocking collectives  30.6 us (19%)
  waiting for transfers between devices  20 us (12%)
  matrix products  17.2 us (11%)
  starting transfers between devices  15.3 us (9%)
  between operations  14.2 us (9%)
  local copies, waits for them, and re-layouts  9.91 us (6%)
  other arithmetic  2.28 us (1%)
    pallas_call x1, Pallas kernels, dispatch(): pl.pallas_call(functools.partial(dispatch_kernel, n, m, cap), in_specs=vm...  36.2 us
    all_to_all x1, blocking collectives, body(): lax.all_to_all(jnp.broadcast_to(mix_rows[None], (experts, values, tok_row...  24.1 us
    pallas_call x3, Pallas kernels, per_head(): pl.pallas_call(kernel, grid=(heads,), in_specs=in_specs, out_specs=[spec(...  15.7 us
    all_to_all x1, waiting for transfers between devices, body(): lax.all_to_all(summed, 'sp', split_axis=0, concat_axis=0, tiled=True)  11.4 us
    reduce_scatter x1, waiting for transfers between devices, body(): lax.psum_scatter(partial_value.astype(BF16), 'tp', scatter_dimension=1, t...  8.61 us
    all_gather x1, blocking collectives, body(): full_rows = lax.all_gather(grad_rows, 'tp', axis=1, tiled=True)  6.5 us
    all_to_all x1, starting transfers between devices, body(): lax.all_to_all(full_rows.reshape(tok_rows, experts, rows_block).swapaxes(...  6 us
    all_to_all x1, starting transfers between devices, body(): lax.all_to_all(summed, 'sp', split_axis=0, concat_axis=0, tiled=True)  5.52 us
  transfers between devices with their start and end apart: 4, of which 2 were waited for; matrix products, arithmetic and copies ran while one was open for 12% of the time, Pallas kernels for 8%

profile of v1, /device:TPU:0, one launch (start us, length us, event | category | flops | bytes accessed | tf_op | source)
XLA Modules:
  0.0 161.4 jit_solution(11564143567103473875)
XLA Ops:
  7.2 36.2 %dispatch.1 = (bf16[2,4,384,512]{3,2,1,0:T(8,128)(2,1)}, bf16[384,512]{1,0:T(8,128)(2,1)}, bf16[384,512]{1,0:T(8,128)(2,1)}, bf16[384,512]{1,0:T(8,128)(2,1)}, b...) custom-call(bf16[128,128]{1,0:T(8,128)(2,1)} %q_ref.5, ...), custom_call_target="tpu_custom_call" | custom-call | tf_op jit(solution)/shard_map/dispatch/pallas_call | solution.py:340
  43.5 2.1 %fusion.6 = f32[384,2048]{1,0:T(8,128)S(1)} fusion(bf16[384,512]{1,0:T(8,128)(2,1)} %get-tuple-element.36, bf16[1,2048,512]{2,1,0:T(8,128)(2,1)S(1)} %copy-done.2), kind=kOutput, calls=%fused_computation.20 | convolution fusion | flops 805306368 | bytes 5636096 | tf_op jit(solution)/shard_map/dot_general | solution.py:509
  45.7 2.2 %add_convert_fusion = bf16[384,2048]{1,0:T(8,128)(2,1)} fusion(f32[384,2048]{1,0:T(8,128)S(1)} %fusion.6, bf16[384,512]{1,0:T(8,128)(2,1)S(1)} %copy-done.6, bf16[1,2048,512]{2,1,0:T(8,128)(2,1)S(1)} %copy-done.1), kind=kOutput, calls=%fused_computation | convolution fusion | flops 806879232 | bytes 7208960 | tf_op jit(solution)/shard_map/dot_general | solution.py:510
  48.1 24.1 %all_to_all.20 = bf16[8,256,128]{1,2,0:T(8,128)(2,1)S(1)} all-to-all(bf16[8,256,128]{1,2,0:T(8,128)(2,1)S(1)} %broadcast_in_dim.48), channel_id=1, replica_groups=mesh['sp'=8,'tp'=4] {'sp'}, dimensions={0} | all-to-all | bytes 1048576 | tf_op jit(solution)/shard_map/all_to_all | solution.py:507
  72.2 8.6 %reduce-scatter.2.cloned.1.call-done = bf16[384,512]{1,0:T(8,128)(2,1)} async-done(((bf16[384,2048]{1,0:T(8,128)(2,1)}), bf16[384,512]{1,0:T(8,128)(2,1)}) %reduce-scatter.2.cloned.1.call-update) | async-done | bytes 393232 | tf_op jit(solution)/shard_map/reduce_scatter | solution.py:513
  80.8 5.5 %all-to-all-start.1 = ((bf16[8,48,512]{2,1,0:T(8,128)(2,1)}), bf16[8,48,512]{2,1,0:T(8,128)(2,1)S(1)}, u32[]{:S(2)}, u32[]{:S(2)}) async-start(bf16[8,48,512]{2,1,0:T(8,128)(2,1)} %bitcast.70), calls=%async_computation.2 | async-start | bytes 786432 | tf_op jit(solution)/shard_map/all_to_all | solution.py:520
  86.4 11.4 %all-to-all-done.1 = bf16[8,48,512]{2,1,0:T(8,128)(2,1)S(1)} async-done(((bf16[8,48,512]{2,1,0:T(8,128)(2,1)}), bf16[8,48,512]{2,1,0:T(8,128)(2,1)S(1)}, u32[]{:S(2)}, u32[]{:S(2)}) %all-to-all-start.1) | async-done | bytes 393248 | tf_op jit(solution)/shard_map/all_to_all | solution.py:520
  98.1 6.5 %all_gather.3 = bf16[128,2048]{1,0:T(8,128)(2,1)S(1)} all-gather(bf16[128,512]{1,0:T(8,128)(2,1)S(1)} %fusion.3), channel_id=1, replica_groups=mesh['sp'=8,'tp'=4] {'tp'}, dimensions={1}, use_global_device_ids=true | all-gather | bytes 655360 | tf_op jit(solution)/shard_map/all_gather | solution.py:523
  104.6 1.2 convolution_bitcast_fusion.1.gn_ref
  105.8 3.2 %shard_map.197 = (f32[256,128]{1,0:T(8,128)}, bf16[128,128]{1,0:T(8,128)(2,1)}, bf16[128,128]{1,0:T(8,128)(2,1)}) custom-call(f32[256,128]{1,0:T(8,128)} %convolution_bitcast_fusion.1.gn_ref, f32[256,128]{1,0:T(8,128)} %get-tuple-element.40.normed_ref, f32[32,128]{1,0:T(8,128)} %get-tuple-element.41.inv_ref, bf16[128,128]{1,0:T(8,128)(2,1)} %q_ref.5, ...), custom_call_target="tpu_custom_call" | custom-call | flops 268435456 | bytes 1048576 | tf_op jit(solution)/shard_map/pallas_call | solution.py:452
  109.0 1.6 broadcast_select_fusion
  110.5 3.7 %all-to-all-start.2 = ((bf16[8,128,128]{2,1,0:T(8,128)(2,1)}), bf16[8,128,128]{2,1,0:T(8,128)(2,1)S(1)}, u32[]{:S(2)}, u32[]{:S(2)}) async-start(bf16[8,128,128]{2,1,0:T(8,128)(2,1)} %broadcast_select_fusion), calls=%async_computation.3 | async-start | bytes 524288 | tf_op jit(solution)/shard_map/all_to_all | solution.py:530
  115.0 8.5 %shard_map.198 = (f32[128,128]{1,0:T(8,128)}, f32[128,128]{1,0:T(8,128)}, f32[256,128]{1,0:T(8,128)}, f32[128,128]{1,0:T(8,128)}, f32[128,128]{1,0:T(8,128)}) custom-call(f32[256,128]{1,0:T(8,128)} %get-tuple-element.43.dm_ref, bf16[128,128]{1,0:T(8,128)(2,1)} %q_ref.5, bf16[128,128]{1,0:T(8,128)(2,1)} %k_ref.5, bf16[256,128]{1,0:T(8,128)(2,1)} %v_ref.5, ...), custom_call_target="tpu_custom_call" | custom-call | flops 2147483648 | bytes 1048576 | tf_op jit(solution)/shard_map/pallas_call | solution.py:452
  123.4 1.0 copy.39
  124.4 6.0 %all-to-all-start.3 = ((bf16[8,128,256]{1,2,0:T(8,128)(2,1)}), bf16[8,128,256]{1,2,0:T(8,128)(2,1)}, u32[]{:S(2)}, u32[]{:S(2)}) async-start(bf16[8,128,256]{1,2,0:T(8,128)(2,1)} %bitcast.17), calls=%async_computation.4 | async-start | bytes 1048576 | tf_op jit(solution)/shard_map/all_to_all | solution.py:540
  130.4 3.3 %slice_bitcast_fusion = (bf16[384,4,512]{2,0,1:T(8,128)(2,1)}, bf16[384,4,512]{2,0,1:T(8,128)(2,1)S(1)}) fusion(bf16[2,4,384,512]{3,2,1,0:T(8,128)(2,1)} %get-tuple-element.60), kind=kLoop, calls=%fused_computation.7 | loop fusion | bytes 6291456 | tf_op jit(solution)/shard_map/transpose | solution.py:500
  133.8 1.0 copy.33
  135.5 1.6 copy.36
  137.1 1.9 %copy.37 = bf16[384,4,512]{0,2,1:T(8,128)(2,1)S(1)} copy(bf16[384,4,512]{2,0,1:T(8,128)(2,1)} %get-tuple-element.62) | data formatting | bytes 3145728 | tf_op jit(solution)/shard_map/transpose | solution.py:500
  139.1 4.1 %fusion = bf16[1,2048,512]{2,1,0:T(8,128)(2,1)} fusion(bf16[384,2048]{0,1:T(8,128)(2,1)} %bitcast.67, bf16[384,512]{1,0:T(8,128)(2,1)S(1)} %copy-done.9), kind=kOutput, calls=%fused_computation.4 | convolution fusion | flops 806354944 | bytes 4063232 | tf_op jit(solution)/shard_map/dot_general | solution.py:517
  143.2 2.6 %fusion.1 = bf16[1,2048,512]{2,1,0:T(8,128)(2,1)} fusion(bf16[384,2048]{0,1:T(8,128)(2,1)S(1)} %bitcast.68, bf16[384,512]{1,0:T(8,128)(2,1)S(1)} %copy-done.7), kind=kOutput, calls=%fused_computation.5 | convolution fusion | flops 806354944 | bytes 4063232 | tf_op jit(solution)/shard_map/dot_general | solution.py:518
  145.8 2.6 %fusion.2 = bf16[1,512,2048]{2,1,0:T(8,128)(2,1)} fusion(bf16[384,512]{1,0:T(8,128)(2,1)S(1)} %copy-done.8, bf16[384,2048]{0,1:T(8,128)(2,1)S(1)} %bitcast.64), kind=kOutput, calls=%fused_computation.6 | convolution fusion | flops 806354944 | bytes 4063232 | tf_op jit(solution)/shard_map/dot_general | solution.py:516
  148.4 4.1 %shard_map.199 = (f32[128,128]{1,0:T(8,128)}, f32[256,128]{1,0:T(8,128)}, f32[128,128]{1,0:T(8,128)}) custom-call(s32[1]{0:T(128)} %bitcast.13.me_ref, bf16[8,128,128]{2,1,0:T(8,128)(2,1)} %copy-done.4, f32[8,128,8]{2,1,0:T(8,128)} %bitcast.66, f32[128,128]{1,0:T(8,128)} %pad_maximum_fusion.carried_ref, bf16[128,128]{1,0:T(8,128)(2,1)} %k_ref.5, ...), custom_call_target="tpu_custom_call" | custom-call | flops 268435456 | bytes 1048576 | tf_op jit(solution)/shard_map/pallas_call | solution.py:452
  152.5 2.0 %convolution_bitcast_fusion = f32[256,256]{1,0:T(8,128)} fusion(bf16[8,128,256]{1,2,0:T(8,128)(2,1)} %all-to-all-done.3, bf16[8,256,128]{1,2,0:T(8,128)(2,1)S(1)} %all_to_all.20), kind=kOutput, calls=%fused_computation.9 | convolution fusion | flops 134217728 | bytes 1310720 | tf_op jit(solution)/shard_map/dot_general | solution.py:542
  (42 shorter events, 2.1 us)
Async XLA Ops:
  7.2 97.4 %copy-start = (bf16[2048,256]{1,0:T(8,128)(2,1)S(1)}, bf16[2048,256]{1,0:T(8,128)(2,1)}, u32[]{:S(2)}) copy-start(bf16[2048,256]{1,0:T(8,128)(2,1)} %param.20) | copy-start | bytes 3145732
  7.2 73.6 %reduce-scatter.2.cloned.1.call-start = ((), (), s32[]{:S(2)}) async-start(), calls=%async_computation.5 | async-start | bytes 1966080 | tf_op jit(solution)/shard_map/reduce_scatter | solution.py:513
  7.2 36.2 %copy-start.2 = (bf16[1,2048,512]{2,1,0:T(8,128)(2,1)S(1)}, bf16[1,2048,512]{2,1,0:T(8,128)(2,1)}, u32[]{:S(2)}) copy-start(bf16[1,2048,512]{2,1,0:T(8,128)(2,1)} %param.25) | copy-start | bytes 6291460
  43.5 2.2 %copy-start.1 = (bf16[1,2048,512]{2,1,0:T(8,128)(2,1)S(1)}, bf16[1,2048,512]{2,1,0:T(8,128)(2,1)}, u32[]{:S(2)}) copy-start(bf16[1,2048,512]{2,1,0:T(8,128)(2,1)} %param.26) | copy-start | bytes 6291460
  43.5 2.2 %copy-start.6 = (bf16[384,512]{1,0:T(8,128)(2,1)S(1)}, bf16[384,512]{1,0:T(8,128)(2,1)}, u32[]{:S(2)}) copy-start(bf16[384,512]{1,0:T(8,128)(2,1)} %get-tuple-element.37) | copy-start | bytes 1179652
  45.7 2.3 %copy-start.12 = (bf16[256,128]{1,0:T(8,128)(2,1)S(1)}, bf16[256,128]{1,0:T(8,128)(2,1)}, u32[]{:S(2)}) copy-start(bf16[256,128]{1,0:T(8,128)(2,1)} %get-tuple-element.38) | copy-start | bytes 196612
  47.9 38.4 %copy-start.11 = (f32[2,64,128]{2,1,0:T(8,128)S(1)}, f32[2,64,128]{2,1,0:T(8,128)}, u32[]{:S(2)}) copy-start(f32[2,64,128]{2,1,0:T(8,128)} %get-tuple-element.45) | copy-start | bytes 196612
  47.9 49.9 %copy-start.5 = (bf16[128,512]{1,0:T(8,128)(2,1)S(1)}, bf16[128,512]{1,0:T(8,128)(2,1)}, u32[]{:S(2)}) copy-start(bf16[128,512]{1,0:T(8,128)(2,1)} %cot_ref.1) | copy-start | bytes 393220
  47.9 49.9 %copy-start.10 = (bf16[384,128]{1,0:T(8,128)(2,1)S(1)}, bf16[384,128]{1,0:T(8,128)(2,1)}, u32[]{:S(2)}) copy-start(bf16[384,128]{1,0:T(8,128)(2,1)} %get-tuple-element.35) | copy-start | bytes 294916
  80.8 17.1 %all-to-all-start.1 = ((bf16[8,48,512]{2,1,0:T(8,128)(2,1)}), bf16[8,48,512]{2,1,0:T(8,128)(2,1)S(1)}, u32[]{:S(2)}, u32[]{:S(2)}) async-start(bf16[8,48,512]{2,1,0:T(8,128)(2,1)} %bitcast.70), calls=%async_computation.2 | async-start | bytes 786432 | tf_op jit(solution)/shard_map/all_to_all | solution.py:520
  110.5 13.9 %all-to-all-start.2 = ((bf16[8,128,128]{2,1,0:T(8,128)(2,1)}), bf16[8,128,128]{2,1,0:T(8,128)(2,1)S(1)}, u32[]{:S(2)}, u32[]{:S(2)}) async-start(bf16[8,128,128]{2,1,0:T(8,128)(2,1)} %broadcast_select_fusion), calls=%async_computation.3 | async-start | bytes 524288 | tf_op jit(solution)/shard_map/all_to_all | solution.py:530
  124.4 9.4 %copy-start.4 = (bf16[8,128,128]{2,1,0:T(8,128)(2,1)}, bf16[8,128,128]{2,1,0:T(8,128)(2,1)S(1)}, u32[]{:S(2)}) copy-start(bf16[8,128,128]{2,1,0:T(8,128)(2,1)S(1)} %all-to-all-done.2.recv_ref) | copy-start | bytes 786436
  124.4 28.1 %all-to-all-start.3 = ((bf16[8,128,256]{1,2,0:T(8,128)(2,1)}), bf16[8,128,256]{1,2,0:T(8,128)(2,1)}, u32[]{:S(2)}, u32[]{:S(2)}) async-start(bf16[8,128,256]{1,2,0:T(8,128)(2,1)} %bitcast.17), calls=%async_computation.4 | async-start | bytes 1048576 | tf_op jit(solution)/shard_map/all_to_all | solution.py:540
  130.4 3.4 %copy-start.13 = (f32[8,8,128]{2,1,0:T(8,128)S(1)}, f32[8,8,128]{2,1,0:T(8,128)}, u32[]{:S(2)}) copy-start(f32[8,8,128]{2,1,0:T(8,128)} %get-tuple-element.49) | copy-start | bytes 98308
  130.4 4.4 %copy-start.14 = (f32[128]{0:T(128)S(1)}, f32[128]{0:T(128)}, u32[]{:S(2)}) copy-start(f32[128]{0:T(128)} %param.19) | copy-start | bytes 1540
  137.1 2.0 %copy-start.9 = (bf16[384,512]{1,0:T(8,128)(2,1)S(1)}, bf16[384,512]{1,0:T(8,128)(2,1)}, u32[]{:S(2)}) copy-start(bf16[384,512]{1,0:T(8,128)(2,1)} %get-tuple-element.36) | copy-start | bytes 1179652
  139.1 4.1 %copy-start.3 = (bf16[384,4,512]{0,2,1:T(8,128)(2,1)S(1)}, bf16[384,4,512]{0,2,1:T(8,128)(2,1)}, u32[]{:S(2)}) copy-start(bf16[384,4,512]{0,2,1:T(8,128)(2,1)} %copy.36) | copy-start | bytes 4718596
  139.1 4.1 %copy-start.7 = (bf16[384,512]{1,0:T(8,128)(2,1)S(1)}, bf16[384,512]{1,0:T(8,128)(2,1)}, u32[]{:S(2)}) copy-start(bf16[384,512]{1,0:T(8,128)(2,1)} %get-tuple-element.37) | copy-start | bytes 1179652
  143.2 2.6 %copy-start.8 = (bf16[384,512]{1,0:T(8,128)(2,1)S(1)}, bf16[384,512]{1,0:T(8,128)(2,1)}, u32[]{:S(2)}) copy-start(bf16[384,512]{1,0:T(8,128)(2,1)} %get-tuple-element.61) | copy-start | bytes 1179652
Sparse Core Ops, SparseCore 0:
  48.0 32.6 reduce-scatter.1

commit v2 on v1

--- a/solution.py
+++ b/solution.py
@@ -357,107 +357,386 @@
     )(q, k, v, pre, extra, speed, x, cot, picks, comb, gate, up, down)
 
 
-def source_kernel(gn_ref, normed_ref, inv_ref, q_ref, cum_ref, dm_ref, fwd_ref, bwd_ref):
-    length = q_ref.shape[1]
-    normed = normed_ref[...]
-    gn = gn_ref[...]
-    dm = inv_ref[0:1, :] * (gn - normed * jnp.mean(gn * normed, axis=0, keepdims=True))
-    dm_ref[...] = dm
-    q = q_ref[...].astype(F32) * KEY_DIM ** (-0.5)
+def combine_kernel(n, m, cap, rows_ref, hidden_ref, ggp_ref, gup_ref, place_ref, cot_ref, mix_ref,
+                   gate_any, up_any,
+                   full_ref, dgate_ref, dup_ref, ddown_ref, all_mix_ref,
+                   gate_v, up_v, own_ref, psend, pin, ybuf, yin, zbuf, ret_ref,
+                   ps, pr, ys, yr, zs, zr, fs, fr, ms, mr, ws):
+    at = Peers(n, m)
+    me = at.me
+    width = cot_ref.shape[1]
+    at.greet()
+    loads = [pltpu.make_async_copy(src, dst, ws.at[i])
+             for i, (src, dst) in enumerate(((gate_any, gate_v), (up_any, up_v)))]
+    for load in loads:
+        load.start()
+
+    def rows(p):
+        return pl.ds(pl.multiple_of(p * cap, 16), cap)
+
+    def partial(j):
+        block = pl.ds(pl.multiple_of(j * width, width), width)
+        return dot(ggp_ref[...], gate_v[block, :], NT) + dot(gup_ref[...], up_v[block, :], NT)
+
+    def pair(dy):
+        return copy_to(psend.at[dy], pin.at[dy], ps.at[dy], pr.at[dy], {"tp": at.mate})
+
+    def column_of(dy, core):
+        return lax.rem(at.chip + dy, at.chips) * CORES + core
+
+    def across(d, dy):
+        r = rows(at.to(d))
+        return copy_to(ybuf.at[dy, r], yin.at[dy, r], ys.at[dy, d], yr.at[dy, d],
+                       {"tp": at.to_chip(dy)})
+
+    def across_in(d, dy):
+        r = rows(at.to(d))
+        return copy_to(yin.at[dy, r], yin.at[dy, r], ys.at[dy, d], yr.at[dy, d],
+                       {"tp": at.from_chip(dy)})
+
+    def back(d):
+        return copy_to(zbuf.at[rows(at.to(d))], ret_ref.at[rows(me)], zs.at[d], zr.at[d],
+                       {"sp": at.to(d)})
+
+    def back_in(d):
+        here = ret_ref.at[rows(at.source(d))]
+        return copy_to(here, here, zs.at[d], zr.at[d], {"sp": at.source(d)})
+
+    def mix_out(d):
+        return copy_to(mix_ref, all_mix_ref.at[me], ms.at[d], mr.at[d], {"sp": at.to(d)})
+
+    def mix_in(d):
+        p = at.source(d)
+        return copy_to(mix_ref, all_mix_ref.at[p], ms.at[d], mr.at[d], {"sp": p})
+
+    all_mix_ref[me] = mix_ref[...]
+    loads[0].wait()
+    loads[1].wait()
+    order = list(range(1, at.chips)) + [0]
+    for i, dy in enumerate(order):
+        psend[dy] = partial(column_of(dy, 1 - at.core)).astype(BF16)
+        if i == 0:
+            at.met()
+        pair(dy).start()
+        if i == 0:
+            loop(n - 1, lambda i: mix_out(i + 1).start())
+        own_ref[dy] = partial(column_of(dy, at.core))
+        if dy > 0:
+            pair(dy).wait_recv()
+            ybuf[dy] = (own_ref[dy] + pin[dy].astype(F32)).astype(BF16)
+            loop(n, lambda d, dy=dy: across(lax.rem(d + 1, n), dy).start())
+    pair(0).wait_recv()
+    own_ref[0] = own_ref[0] + pin[0].astype(F32)
+
+    pieces = []
+    for j in range(m):
+        cols = slice(j * width, (j + 1) * width)
+
+        def gate_piece(j=j, cols=cols):
+            dgate_ref[cols, :] = dot(rows_ref[0, j], ggp_ref[...], TN).astype(BF16)
+
+        def up_piece(j=j, cols=cols):
+            dup_ref[cols, :] = dot(rows_ref[0, j], gup_ref[...], TN).astype(BF16)
+
+        def down_piece(j=j, cols=cols):
+            ddown_ref[:, cols] = dot(hidden_ref[...], rows_ref[1, j], TN).astype(BF16)
+        pieces += [gate_piece, up_piece, down_piece]
+
+    steps = n + 4
+    done = 0
+    for i in range(n):
+        upto = len(pieces) * (i + 1) // steps
+        for piece in pieces[done:upto]:
+            piece()
+        done = upto
+        d = (i + 1) % n
+        r = rows(at.to(d))
+        total = own_ref[0, r, :]
+        for dy in range(1, at.chips):
+            across_in(d, dy).wait_recv()
+            total = total + yin[dy, r, :].astype(F32)
+        if d == 0:
+            ret_ref[r, :] = total.astype(BF16)
+        else:
+            zbuf[r, :] = total.astype(BF16)
+            back(d).start()
+    upto = len(pieces) * (n + 2) // steps
+    for piece in pieces[done:upto]:
+        piece()
+    loop(n - 1, lambda i: back_in(i + 1).wait_recv())
+    picked = dot(place_ref[...], ret_ref[...], TN)
+    full_ref[at.tp] = (cot_ref[...].astype(F32) + picked).astype(BF16)
+
+    def share(dy):
+        here = full_ref.at[at.tp]
+        return copy_to(here, here, fs.at[0, dy], fr.at[0, dy],
+                       {"tp": at.to_chip(dy)} if dy else {"tp": at.mate})
+
+    def share_in(dy):
+        here = full_ref.at[at.from_chip(dy) if dy else at.mate]
+        return copy_to(here, here, fs.at[0, dy], fr.at[0, dy], {"tp": at.mate})
+
+    def relay(dy):
+        here = full_ref.at[at.from_chip(dy)]
+        return copy_to(here, here, fs.at[1, dy], fr.at[1, dy], {"tp": at.mate})
+
+    def relay_in(dy):
+        here = full_ref.at[at.mate_from_chip(dy)]
+        return copy_to(here, here, fs.at[1, dy], fr.at[1, dy], {"tp": at.mate})
+
+    for dy in order:
+        share(dy).start()
+    for piece in pieces[upto:]:
+        piece()
+    for dy in range(1, at.chips):
+        share_in(dy).wait_recv()
+        relay(dy).start()
+    share_in(0).wait_recv()
+    for dy in range(1, at.chips):
+        relay_in(dy).wait_recv()
+    for dy in range(at.chips):
+        pair(dy).wait_send()
+        share(dy).wait_send()
+    for dy in range(1, at.chips):
+        relay(dy).wait_send()
+        loop(n, lambda d, dy=dy: across(d, dy).wait_send())
+    loop(n - 1, lambda i: back(i + 1).wait_send())
+    loop(n - 1, lambda i: mix_out(i + 1).wait_send())
+    loop(n - 1, lambda i: mix_in(i + 1).wait_recv())
+
+
+def combine(n, m, cap, rows, hidden, ggp, gup, place, cot, mix, gate, up):
+    slots, units = hidden.shape
+    tok, width = cot.shape
+    chips = m // CORES
+    dma = pltpu.SemaphoreType.DMA
+    outs = [((m, tok, width), BF16), (gate.shape, BF16), (up.shape, BF16),
+            ((units, m * width), BF16), ((n,) + mix.shape, BF16)]
+    return pl.pallas_call(
+        functools.partial(combine_kernel, n, m, cap),
+        in_specs=vmem_specs(7) + [pl.BlockSpec(memory_space=pl.ANY)] * 2,
+        out_specs=vmem_specs(len(outs)),
+        out_shape=[jax.ShapeDtypeStruct(shape, dtype) for shape, dtype in outs],
+        scratch_shapes=[
+            pltpu.VMEM(gate.shape, BF16), pltpu.VMEM(up.shape, BF16),
+            pltpu.VMEM((chips, slots, width), F32), pltpu.VMEM((chips, slots, width), BF16),
+            pltpu.VMEM((chips, slots, width), BF16), pltpu.VMEM((chips, slots, width), BF16),
+            pltpu.VMEM((chips, slots, width), BF16), pltpu.VMEM((slots, width), BF16),
+            pltpu.VMEM((slots, width), BF16),
+            dma((chips,)), dma((chips,)), dma((chips, n)), dma((chips, n)), dma((n,)), dma((n,)),
+            dma((2, chips)), dma((2, chips)), dma((n,)), dma((n,)), dma((2,)),
+        ],
+        compiler_params=pltpu.CompilerParams(collective_id=1, has_side_effects=True,
+                                             vmem_limit_bytes=VMEM_LIMIT),
+        name="combine",
+    )(rows, hidden, ggp, gup, place, cot, mix, gate, up)
+
+
+def finish_kernel(n, m, project, *refs):
+    (full_ref, wo_ref, normed_ref, inv_ref, q_ref, k_ref, v_ref, pre_ref, speed_ref, cum_ref,
+     st_ref, carried_ref, last_ref) = refs[:13]
+    refs = refs[13:]
+    if project:
+        mix_ref, refs = refs[0], refs[1:]
+    dq_ref, dk_ref, dv_ref, logit_ref = refs[:4]
+    refs = refs[4:]
+    if project:
+        proj_ref, refs = refs[0], refs[1:]
+    dm_ref, dc_ref, sbuf, sin, ss, sr = refs[:6]
+    if project:
+        psend, prow, zs, zr, fs, fr = refs[6:]
+    at = Peers(n, m)
+    me = at.me
+    channels, tok = q_ref.shape
+    values = v_ref.shape[0]
+    heads = channels // KEY_DIM
+    width = full_ref.shape[2]
+    at.greet()
+
+    def exchange(d):
+        p = at.to(d)
+        return copy_to(sbuf.at[jnp.where(p < me, 0, 1)], sin.at[me], ss.at[d], sr.at[d],
+                       {"sp": p})
+
+    def exchange_in(d):
+        p = at.source(d)
+        return copy_to(sbuf.at[0], sin.at[p], ss.at[d], sr.at[d], {"sp": p})
+
+    gn = None
+    for j in range(m):
+        part = dot(full_ref[j], wo_ref[j * width:(j + 1) * width, :], NN)
+        gn = part if gn is None else gn + part
+    gn = gn.T
+    for h in range(heads):
+        block = slice(h * VAL_DIM, (h + 1) * VAL_DIM)
+        normed, g = normed_ref[block, :], gn[block]
+        dm_ref[block, :] = inv_ref[h * 8:h * 8 + 1, :] * (
+            g - normed * jnp.mean(g * normed, axis=0, keepdims=True))
     cum = cum_ref[...]
-    last = cum[:, length - 1:length]
-    fwd = dot(q * jnp.exp(cum), dm, ((1,), (1,)))
-    bwd = dot(q * jnp.exp(last - cum), dm, ((1,), (1,)))
-    pad = jnp.zeros_like(fwd)
-    fwd_ref[...] = jnp.concatenate([fwd, pad], axis=1).astype(BF16)
-    bwd_ref[...] = jnp.concatenate([bwd, pad], axis=1).astype(BF16)
-
-
-def inner_kernel(dm_ref, q_ref, k_ref, v_ref, cum_ref, st_ref, carried_ref,
-                 dq_ref, dk_ref, dv_ref, dc_ref, dt_ref):
-    length = q_ref.shape[1]
+    last = cum[:, tok - 1:tok]
+    up, down = jnp.exp(cum), jnp.exp(last - cum)
+    scale = KEY_DIM ** (-0.5)
+    q = q_ref[...].astype(F32) * scale
     dm = dm_ref[...]
-    q = q_ref[...].astype(F32) * KEY_DIM ** (-0.5)
+    sbuf[0] = own_heads(dot(dm, q * up, NT), VAL_DIM).astype(BF16)
+    sbuf[1] = own_heads(dot(dm, q * down, NT), VAL_DIM).astype(BF16)
+    sin[me] = jnp.zeros(sin.shape[1:], BF16)
+    if project:
+        block = proj_ref.shape[0]
+        share = tok // m
+        row = lax.broadcasted_iota(jnp.int32, (share, tok), 0) + at.tp * share
+        chosen = (row == lax.broadcasted_iota(jnp.int32, (share, tok), 1)).astype(BF16)
+        per = width // block
+        for j in range(m):
+            part = dot(chosen, full_ref[j], NN).astype(BF16)
+            for i in range(per):
+                psend[j * per + i] = part[:, i * block:(i + 1) * block]
+
+        def share_of(j):
+            return pl.ds(pl.multiple_of(j * share, 16), share)
+
+        def rows_out(d):
+            p = at.to(d)
+            return copy_to(psend.at[p], prow.at[me, share_of(at.tp)], zs.at[d], zr.at[d],
+                           {"sp": p})
+
+        def rows_in(d):
+            here = prow.at[at.source(d), share_of(at.tp)]
+            return copy_to(here, here, zs.at[d], zr.at[d], {"sp": at.source(d)})
+
+        def spread(dy):
+            here = prow.at[:, share_of(at.tp)]
+            return copy_to(here, here, fs.at[0, dy], fr.at[0, dy],
+                           {"tp": at.to_chip(dy)} if dy else {"tp": at.mate})
+
+        def spread_in(dy):
+            here = prow.at[:, share_of(at.from_chip(dy) if dy else at.mate)]
+            return copy_to(here, here, fs.at[0, dy], fr.at[0, dy], {"tp": at.mate})
+
+        def relay(dy):
+            here = prow.at[:, share_of(at.from_chip(dy))]
+            return copy_to(here, here, fs.at[1, dy], fr.at[1, dy], {"tp": at.mate})
+
+        def relay_in(dy):
+            here = prow.at[:, share_of(at.mate_from_chip(dy))]
+            return copy_to(here, here, fs.at[1, dy], fr.at[1, dy], {"tp": at.mate})
+
+        prow[me, share_of(at.tp), :] = psend[me]
+    at.met()
+    loop(n - 1, lambda i: exchange(i + 1).start())
+    if project:
+        loop(n - 1, lambda i: rows_out(i + 1).start())
+
+    row = lax.broadcasted_iota(jnp.int32, (tok, tok), 0)
+    col = lax.broadcasted_iota(jnp.int32, (tok, tok), 1)
+    sign = jnp.where(row > col, 1.0, jnp.where(row < col, -1.0, 0.0)).astype(F32)
+
+    def head(h):
+        keys = pl.ds(pl.multiple_of(h * KEY_DIM, KEY_DIM), KEY_DIM)
+        vals = pl.ds(pl.multiple_of(h * VAL_DIM, VAL_DIM), VAL_DIM)
+        dm, v, cum = dm_ref[vals, :], v_ref[vals, :], cum_ref[keys, :]
+        q = q_ref[keys, :].astype(F32) * scale
+        k = k_ref[keys, :].astype(F32)
+        by_query = dot(dm, v, TN)
+        by_key = dot(v, dm, TN)
+        by_query_signed = by_query * sign
+        by_key_signed = by_key * -sign
+        cum_t, q_t, k_t = cum.T, q.T, k.T
+        dq, dk, dq_signed, dk_signed = [], [], [], []
+        for c in range(KEY_DIM):
+            weight = jnp.exp(-jnp.abs(cum_t[:, c:c + 1] - cum[c:c + 1, :]))
+            with_q = weight * q_t[:, c:c + 1]
+            with_k = weight * k_t[:, c:c + 1]
+            dk.append(jnp.sum(by_query * with_q, axis=0, keepdims=True))
+            dk_signed.append(jnp.sum(by_query_signed * with_q, axis=0, keepdims=True))
+            dq.append(jnp.sum(by_key * with_k, axis=0, keepdims=True))
+            dq_signed.append(jnp.sum(by_key_signed * with_k, axis=0, keepdims=True))
+        join = lambda parts: jnp.concatenate(parts, axis=0)
+        dq_ref[keys, :] = join(dq)
+        dk_ref[keys, :] = join(dk)
+        dv_ref[vals, :] = dot(dm, st_ref[pl.ds(pl.multiple_of(h * tok, tok), tok), :], NT)
+        dc_ref[keys, :] = q * join(dq_signed) - k * join(dk_signed)
+
+    early = heads // 2
+    loop(early, head)
+    if project:
+        loop(n - 1, lambda i: rows_in(i + 1).wait_recv())
+        for dy in range(at.chips):
+            spread(dy).start()
+    loop(heads - early, lambda h: head(h + early))
+    if project:
+        for dy in range(1, at.chips):
+            spread_in(dy).wait_recv()
+            relay(dy).start()
+
     k = k_ref[...].astype(F32)
+    in_fwd, in_bwd = carried_ref[0], carried_ref[1]
+    d_up = dot(spread_heads(in_fwd, heads), dm, TN) * up
+    d_down = dot(spread_heads(in_bwd, heads), dm, TN) * down
+    dq_ref[...] = (dq_ref[...] + d_up + d_down) * scale
+    dc = dc_ref[...] + q * (d_up - d_down)
+    total = jnp.sum(q * d_down, axis=1, keepdims=True)
+
+    loop(n - 1, lambda i: exchange_in(i + 1).wait_recv())
+    grad_bwd, grad_fwd = carry(n, me, lambda i: sin[i].astype(F32),
+                               lambda i: jnp.exp(last_ref[i, 0:1, :]))
+    wide_fwd, wide_bwd = spread_heads(grad_fwd, heads), spread_heads(grad_bwd, heads)
     v = v_ref[...]
-    cum = cum_ref[...]
-    by_query = dot(dm, v, ((0,), (0,)))
-    by_key = dot(v, dm, ((0,), (0,)))
-    sign = jnp.where(triangle(length, lambda a, b: a > b), 1.0,
-                     jnp.where(triangle(length, lambda a, b: a < b), -1.0, 0.0)).astype(F32)
-    by_query_signed = by_query * sign
-    by_key_signed = by_key * -sign
-    cum_t, q_t, k_t = cum.T, q.T, k.T
-    dq, dk, dq_signed, dk_signed = [], [], [], []
-    for c in range(KEY_DIM):
-        weight = jnp.exp(-jnp.abs(cum_t[:, c:c + 1] - cum[c:c + 1, :]))
-        with_q = weight * q_t[:, c:c + 1]
-        with_k = weight * k_t[:, c:c + 1]
-        dk.append(jnp.sum(by_query * with_q, axis=0, keepdims=True))
-        dk_signed.append(jnp.sum(by_query_signed * with_q, axis=0, keepdims=True))
-        dq.append(jnp.sum(by_key * with_k, axis=0, keepdims=True))
-        dq_signed.append(jnp.sum(by_key_signed * with_k, axis=0, keepdims=True))
-    join = lambda rows: jnp.concatenate(rows, axis=0)
-    last = cum[:, length - 1:length]
-    carried = carried_ref[...]
-    up, down = jnp.exp(cum), jnp.exp(last - cum)
-    d_up = dot(carried[:, :VAL_DIM], dm, ((1,), (0,))) * up
-    d_down = dot(carried[:, VAL_DIM:], dm, ((1,), (0,))) * down
-    dq_ref[...] = (join(dq) + d_up + d_down) * KEY_DIM ** (-0.5)
-    dk_ref[...] = join(dk)
-    dv_ref[...] = dot(dm, st_ref[...], ((1,), (1,)))
-    dc_ref[...] = q * (join(dq_signed) + d_up - d_down) - k * join(dk_signed)
-    dt_ref[...] = jnp.broadcast_to(
-        jnp.sum(q * d_down, axis=1, keepdims=True), dt_ref.shape)
-
-
-def last_kernel(me_ref, recv_ref, first_ref, carried_ref, k_ref, v_ref, cum_ref,
-                pre_ref, speed_ref, dk_in_ref, dv_in_ref, dc_in_ref, dt_ref,
-                dk_ref, dv_ref, logit_ref):
-    length = k_ref.shape[1]
-    me = me_ref[0]
-    grad_bwd, grad_fwd = carry(
-        recv_ref.shape[0], me, lambda i: recv_ref[i, :, :VAL_DIM].astype(F32),
-        lambda i: jnp.exp(first_ref[i, :, 0:1]))
-    k = k_ref[...].astype(F32)
-    v = v_ref[...]
-    cum = cum_ref[...]
-    last = cum[:, length - 1:length]
-    up, down = jnp.exp(cum), jnp.exp(last - cum)
-    d_down = dot(grad_fwd, v, ((1,), (0,))) * down
-    d_up = dot(grad_bwd, v, ((1,), (0,))) * up
-    dk_ref[...] = dk_in_ref[...] + d_down + d_up
-    dv_ref[...] = (dv_in_ref[...] + dot(grad_fwd, k * down, ((0,), (0,)))
-                   + dot(grad_bwd, k * up, ((0,), (0,))))
-    carried = carried_ref[...]
-    grad_factor = jnp.sum(grad_fwd * carried[:, :VAL_DIM] + grad_bwd * carried[:, VAL_DIM:],
-                          axis=1, keepdims=True)
-    grad_total = (dt_ref[:, 0:1] + jnp.sum(k * d_down, axis=1, keepdims=True)
-                  + grad_factor * jnp.exp(last))
-    dc = dc_in_ref[...] + k * (d_up - d_down)
-    from_here = triangle(length, lambda a, b: a >= b).astype(F32)
-    grad_decay = exact_dot(dc, from_here) + grad_total
-    pre = pre_ref[...].astype(F32)
-    logit_ref[...] = grad_decay * speed_ref[...] * jax.nn.sigmoid(-pre)
-
-
-def per_head(kernel, heads, outs, args, vmem_ops, scalars=0):
-    def spec(shape):
-        if len(shape) == 3:
-            return pl.BlockSpec((shape[0], shape[1] // heads, shape[2]), lambda h: (0, h, 0))
-        return pl.BlockSpec((shape[0] // heads, shape[1]), lambda h: (h, 0))
-
-    in_specs = [pl.BlockSpec(memory_space=pltpu.SMEM)] * scalars
-    in_specs += [spec(arg.shape) for arg in args[scalars:]]
+    d_down = dot(wide_fwd, v, TN) * down
+    d_up = dot(wide_bwd, v, TN) * up
+    dk_ref[...] = dk_ref[...] + d_down + d_up
+    dv_ref[...] = dv_ref[...] + dot(wide_fwd, k * down, NN) + dot(wide_bwd, k * up, NN)
+    factor = as_column(jnp.sum(grad_fwd * in_fwd + grad_bwd * in_bwd, axis=0, keepdims=True))
+    total = total + jnp.sum(k * d_down, axis=1, keepdims=True) + factor * jnp.exp(last)
+    dc = dc + k * (d_up - d_down)
+    decay = exact_dot(dc, triangle(tok, lambda a, b: a >= b).astype(F32)) + total
+    logit_ref[...] = decay * as_column(speed_ref[...]) * jax.nn.sigmoid(
+        -pre_ref[...].astype(F32))
+
+    if project:
+        spread_in(0).wait_recv()
+        for dy in range(1, at.chips):
+            relay_in(dy).wait_recv()
+        out = None
+        for s in range(n):
+            part = dot(mix_ref[s], prow[s], NN)
+            out = part if out is None else out + part
+        proj_ref[...] = out.T
+        for dy in range(at.chips):
+            spread(dy).wait_send()
+        for dy in range(1, at.chips):
+            relay(dy).wait_send()
+        loop(n - 1, lambda i: rows_out(i + 1).wait_send())
+    loop(n - 1, lambda i: exchange(i + 1).wait_send())
+
+
+def finish(n, m, project, full, wo, normed, inv, q, k, v, pre, speed, cum, st, carried, lasts,
+           all_mix):
+    channels, tok = q.shape
+    values = v.shape[0]
+    block = wo.shape[0] // n
+    chips = m // CORES
+    dma = pltpu.SemaphoreType.DMA
+    outs = [((channels, tok), F32), ((channels, tok), F32), ((values, tok), F32),
+            ((channels, tok), F32)]
+    scratch = [pltpu.VMEM((values, tok), F32), pltpu.VMEM((channels, tok), F32),
+               pltpu.VMEM((2, VAL_DIM, channels), BF16), pltpu.VMEM((n, VAL_DIM, channels), BF16),
+               dma((n,)), dma((n,))]
+    args = [full, wo, normed, inv, q, k, v, pre, speed, cum, st, carried, lasts]
+    if project:
+        args.append(all_mix)
+        outs.append(((block, values), F32))
+        scratch += [pltpu.VMEM((n, tok // m, block), BF16), pltpu.VMEM((n, tok, block), BF16),
+                    dma((n,)), dma((n,)), dma((2, chips)), dma((2, chips))]
     return pl.pallas_call(
-        kernel,
-        grid=(heads,),
-        in_specs=in_specs,
-        out_specs=[spec(shape) for shape, _ in outs],
+        functools.partial(finish_kernel, n, m, project),
+        in_specs=vmem_specs(len(args)),
+        out_specs=vmem_specs(len(outs)),
         out_shape=[jax.ShapeDtypeStruct(shape, dtype) for shape, dtype in outs],
-        cost_estimate=pl.CostEstimate(
-            flops=vmem_ops * heads, bytes_accessed=1 << 20, transcendentals=0),
-        compiler_params=pltpu.CompilerParams(dimension_semantics=("arbitrary",)),
+        scratch_shapes=scratch,
+        compiler_params=pltpu.CompilerParams(collective_id=2, has_side_effects=True,
+                                             vmem_limit_bytes=VMEM_LIMIT),
+        name="finish",
     )(*args)
 
 
@@ -480,73 +759,33 @@
     heads = input_value_matrix.shape[0] // VAL_DIM
     tok_rows = queries.shape[1]
     experts, m = lax.axis_size("sp"), lax.axis_size("tp")
-    index = lax.axis_index("sp")
-    me = index.astype(jnp.int32).reshape(1)
     capacity = -(-(3 * tok_rows // experts) // 16) * 16
     slots = experts * capacity
     part_width = stored_expert_rows.shape[1]
-    model_width = expert_gate_weight.shape[1]
-    channels = heads * KEY_DIM
-    values = heads * VAL_DIM
-    tn = (((0,), (0,)), ((), ()))
-    nt = (((1,), (1,)), ((), ()))
     gate_local, up_local, down_local = expert_gate_weight[0], expert_up_weight[0], expert_down_weight[0]
     (rows, hidden, grad_gate_pre, grad_up_pre, place, scores, cum, normed, inv_rms, mix_rows,
      carried, lasts) = dispatch(
         experts, m, capacity, queries, input_key_matrix, input_value_matrix,
         decay_preactivation, extra_log_decay, channel_decay_speed[None, :], stored_expert_rows,
         cotangent, chosen_expert_index.T, expert_combine_weight.T, gate_local, up_local, down_local)
-    rows_x = rows[0].swapaxes(0, 1).reshape(slots, m * part_width)
-    rows_dy = rows[1].swapaxes(0, 1).reshape(slots, m * part_width)
-    carried = jnp.concatenate([carried[0].T, carried[1].T], axis=1)
-    sums = lasts.swapaxes(1, 2)
-    place = place.T
-    speed = channel_decay_speed[:, None]
-    state = ((channels, 2 * VAL_DIM), BF16)
-    peer = lax.broadcasted_iota(jnp.int32, (experts, 1, 1), 0)
-    all_mix = lax.all_to_all(jnp.broadcast_to(mix_rows[None], (experts, values, tok_rows)),
-                             "sp", split_axis=0, concat_axis=0, tiled=True)
-    partial_value = lax.dot_general(grad_gate_pre, gate_local, nt, preferred_element_type=F32)
-    partial_value = partial_value + lax.dot_general(
-        grad_up_pre, up_local, nt, preferred_element_type=F32
-    )
-    summed = lax.psum_scatter(
-        partial_value.astype(BF16), "tp", scatter_dimension=1, tiled=True
-    ).reshape(experts, capacity, part_width)
-    grad_down = lax.dot_general(hidden, rows_dy, tn, preferred_element_type=F32).astype(BF16)
-    grad_gate = lax.dot_general(rows_x, grad_gate_pre, tn, preferred_element_type=F32).astype(BF16)
-    grad_up = lax.dot_general(rows_x, grad_up_pre, tn, preferred_element_type=F32).astype(BF16)
-    summed, all_mix = lax.optimization_barrier((summed, all_mix))
-    returned = lax.all_to_all(summed, "sp", split_axis=0, concat_axis=0, tiled=True)
-    picked = jnp.dot(place, returned.reshape(slots, part_width), preferred_element_type=F32)
-    grad_rows = (cotangent.astype(F32) + picked).astype(BF16)
-    full_rows = lax.all_gather(grad_rows, "tp", axis=1, tiled=True)
-    grad_normed = lax.dot_general(
-        output_weight_matrix, full_rows, (((0,), (1,)), ((), ())), preferred_element_type=F32
-    )
-    grad_mixed, fwd_source, bwd_source = per_head(
-        source_kernel, heads, [((values, tok_rows), F32), state, state],
-        [grad_normed, normed, inv_rms, queries, cum], 1 << 26)
-    sources = lax.all_to_all(jnp.where(peer < index, fwd_source[None], bwd_source[None]),
-                             "sp", split_axis=0, concat_axis=0, tiled=True)
-    by_channel = ((channels, tok_rows), F32)
-    grad_queries, dk, dv, dc, dt = per_head(
-        inner_kernel, heads,
-        [by_channel, by_channel, ((values, tok_rows), F32), by_channel, by_channel],
-        [grad_mixed, queries, input_key_matrix, input_value_matrix, cum, scores, carried],
-        1 << 29)
-    full_rows, dk = lax.optimization_barrier((full_rows, dk))
-    rows_block = model_width // experts
-    all_rows = lax.all_to_all(full_rows.reshape(tok_rows, experts, rows_block).swapaxes(0, 1),
-                              "sp", split_axis=0, concat_axis=0, tiled=True)
-    grad_out_proj = lax.dot_general(
-        all_rows.reshape(experts * tok_rows, rows_block),
-        all_mix.swapaxes(1, 2).reshape(experts * tok_rows, values),
-        tn, preferred_element_type=F32)
-    grad_keys, grad_values, grad_logit = per_head(
-        last_kernel, heads, [by_channel, ((values, tok_rows), F32), by_channel],
-        [me, sources, sums, carried, input_key_matrix, input_value_matrix, cum,
-         decay_preactivation, speed, dk, dv, dc, dt], 1 << 26, scalars=1)
+    full, grad_gate, grad_up, grad_down, all_mix = combine(
+        experts, m, capacity, rows, hidden, grad_gate_pre, grad_up_pre, place, cotangent,
+        mix_rows, gate_local, up_local)
+    rows_block = output_weight_matrix.shape[0] // experts
+    project = (tok_rows % (16 * m) == 0 and rows_block % 128 == 0
+               and part_width % rows_block == 0)
+    grads = finish(
+        experts, m, project, full, output_weight_matrix, normed, inv_rms, queries,
+        input_key_matrix, input_value_matrix, decay_preactivation, channel_decay_speed[None, :],
+        cum, scores, carried, lasts, all_mix)
+    grad_queries, grad_keys, grad_values, grad_logit = grads[:4]
+    if project:
+        grad_out_proj = grads[4]
+    else:
+        full_rows = full.swapaxes(0, 1).reshape(tok_rows, experts, rows_block)
+        all_rows = lax.all_to_all(full_rows.swapaxes(0, 1), "sp", split_axis=0, concat_axis=0,
+                                  tiled=True)
+        grad_out_proj = jnp.einsum("str,sct->rc", all_rows, all_mix, preferred_element_type=F32)
     return (
         grad_queries,
         grad_keys,

time: 162 us -> 111 us (0.69)
  Pallas kernels: 52 us -> 96 us
  blocking collectives: 30.6 us -> 0 us
  waiting for transfers between devices: 20 us -> 0 us
  matrix products: 17.2 us -> 0 us
  starting transfers between devices: 15.3 us -> 0 us
  between operations: 14.2 us -> 0.67 us
  local copies, waits for them, and re-layouts: 9.91 us -> 13.7 us
  other arithmetic: 2.28 us -> 0 us
    pallas_call x3 -> x2, Pallas kernels: 15.7 us -> 59.9 us  [the longest x1 38.6 us: combine(): pl.pallas_call(functools.partial(combine_kernel, n, m, cap), in_specs=vme...]
    all_to_all x1 -> x0, blocking collectives: 24.1 us -> none  [body(): lax.all_to_all(jnp.broadcast_to(mix_rows[None], (experts, values, tok_row...]
    dot_general x8 -> x0, matrix products: 17.2 us -> none  [the longest x1 4.11 us: body(): lax.dot_general(rows_x, grad_gate_pre, tn, preferred_element_type=F32)]
    all_to_all x3 -> x0, starting transfers between devices: 15.2 us -> none  [the longest x1 6 us: body(): lax.all_to_all(full_rows.reshape(tok_rows, experts, rows_block).swapaxes(...]
    unnamed x30 -> x14, local copies, waits for them, and re-layouts: 0.07 us -> 13.7 us
    all_to_all x3 -> x0, waiting for transfers between devices: 11.4 us -> none  [the longest x1 11.4 us: body(): lax.all_to_all(summed, 'sp', split_axis=0, concat_axis=0, tiled=True)]
    reduce_scatter x1 -> x0, waiting for transfers between devices: 8.61 us -> none  [body(): lax.psum_scatter(partial_value.astype(BF16), 'tp', scatter_dimension=1, t...]
    transpose x4 -> x0, local copies, waits for them, and re-layouts: 6.84 us -> none  [the longest x2 5.27 us: body(): rows_dy = rows[1].swapaxes(0, 1).reshape(slots, m * part_width)]
  transfers between devices with their start and end apart: 4 -> 0, of which waited for: 2 -> 0; matrix products, arithmetic and copies ran while one was open for 12% -> 0% of each run, Pallas kernels for 8% -> 0%
where the time goes in v2:
time: 111 us; the launch traced here: 110 us
  Pallas kernels  96 us (86%)
  local copies, waits for them, and re-layouts  13.7 us (12%)
    pallas_call x1, Pallas kernels, combine(): pl.pallas_call(functools.partial(combine_kernel, n, m, cap), in_specs=vme...  38.6 us
    pallas_call x1, Pallas kernels, dispatch(): pl.pallas_call(functools.partial(dispatch_kernel, n, m, cap), in_specs=vm...  36.1 us
    pallas_call x1, Pallas kernels, finish(): pl.pallas_call(functools.partial(finish_kernel, n, m, project), in_specs=...  21.3 us
    unnamed x14, local copies, waits for them, and re-layouts  13.7 us

profile of v2, /device:TPU:0, one launch (start us, length us, event | category | flops | bytes accessed | tf_op | source)
XLA Modules:
  0.0 110.4 jit_solution(5603124600567736916)
XLA Ops:
  0.6 36.1 %dispatch.1 = (bf16[2,4,384,512]{3,2,1,0:T(8,128)(2,1)}, bf16[384,512]{1,0:T(8,128)(2,1)}, bf16[384,512]{1,0:T(8,128)(2,1)}, bf16[384,512]{1,0:T(8,128)(2,1)}, b...) custom-call(bf16[128,128]{1,0:T(8,128)(2,1)} %refs_4_.1, ...), custom_call_target="tpu_custom_call" | custom-call | tf_op jit(solution)/shard_map/dispatch/pallas_call | solution.py:340
  36.8 38.6 %combine.1 = (bf16[4,128,512]{2,1,0:T(8,128)(2,1)}, bf16[2048,512]{1,0:T(8,128)(2,1)}, bf16[2048,512]{1,0:T(8,128)(2,1)}, bf16[512,2048]{1,0:T(8,128)(2,1)}, bf16[8,256,128]{2,1,0:T(8,128)(2,1)}) custom-call(bf16[2,4,384,512]{3,2,1,0:T(8,128)(2,1)} %get-tuple-element.30.rows_ref, bf16[384,512]{1,0:T(8,128)(2,1)} %get-tuple-element.31.hidden_ref, ...), custom_call_target="tpu_custom_call" | custom-call | tf_op jit(solution)/shard_map/combine/pallas_call | solution.py:515
  75.4 0.0 copy-start.2
  75.4 21.3 %finish.1 = (f32[128,128]{1,0:T(8,128)}, f32[128,128]{1,0:T(8,128)}, f32[256,128]{1,0:T(8,128)}, f32[128,128]{1,0:T(8,128)}, f32[256,256]{1,0:T(8,128)}) custom-call(bf16[4,128,512]{2,1,0:T(8,128)(2,1)} %get-tuple-element.36.refs_0_, bf16[2048,256]{1,0:T(8,128)(2,1)} %refs_1_.1, f32[256,128]{1,0:T(8,128)} %get-tuple-element.37.refs_2_, ...), custom_call_target="tpu_custom_call" | custom-call | tf_op jit(solution)/shard_map/finish/pallas_call | solution.py:731
  96.7 1.5 %copy.30 = f32[128,128]{1,0:T(8,128)} copy(f32[128,128]{1,0:T(8,128)} %get-tuple-element.60) | data formatting | bytes 131072
  98.2 1.5 %copy.31 = f32[128,128]{1,0:T(8,128)} copy(f32[128,128]{1,0:T(8,128)} %get-tuple-element.61) | data formatting | bytes 131072
  99.6 1.6 %copy.32 = f32[256,128]{1,0:T(8,128)} copy(f32[256,128]{1,0:T(8,128)} %get-tuple-element.62) | data formatting | bytes 262144
  101.2 1.5 %copy.33 = f32[128,128]{1,0:T(8,128)} copy(f32[128,128]{1,0:T(8,128)} %get-tuple-element.63) | data formatting | bytes 131072
  102.7 1.7 %copy.34 = f32[256,256]{1,0:T(8,128)} copy(f32[256,256]{1,0:T(8,128)} %get-tuple-element.64) | data formatting | bytes 524288
  104.3 0.0 copy-done.2
  104.4 0.0 copy-start.1
  104.4 1.3 %copy.35 = bf16[1,2048,512]{2,1,0:T(8,128)(2,1)} copy(bf16[1,2048,512]{2,1,0:T(8,128)(2,1)S(1)} %bitcast.16) | data formatting | bytes 4194304
  105.7 1.0 copy-done.1
  106.7 0.0 copy-start
  106.7 1.3 %copy.36 = bf16[1,2048,512]{2,1,0:T(8,128)(2,1)} copy(bf16[1,2048,512]{2,1,0:T(8,128)(2,1)S(1)} %bitcast.15) | data formatting | bytes 4194304
  108.0 1.0 copy-done
  109.0 1.3 %copy.37 = bf16[1,512,2048]{2,1,0:T(8,128)(2,1)} copy(bf16[1,512,2048]{2,1,0:T(8,128)(2,1)S(1)} %bitcast.14) | data formatting | bytes 4194304
Async XLA Ops:
  75.4 29.0 %copy-start.2 = (bf16[2048,512]{1,0:T(8,128)(2,1)S(1)}, bf16[2048,512]{1,0:T(8,128)(2,1)}, u32[]{:S(2)}) copy-start(bf16[2048,512]{1,0:T(8,128)(2,1)} %get-tuple-element.49) | copy-start | bytes 6291460
  104.4 2.3 %copy-start.1 = (bf16[2048,512]{1,0:T(8,128)(2,1)S(1)}, bf16[2048,512]{1,0:T(8,128)(2,1)}, u32[]{:S(2)}) copy-start(bf16[2048,512]{1,0:T(8,128)(2,1)} %get-tuple-element.50) | copy-start | bytes 6291460
  106.7 2.3 %copy-start = (bf16[512,2048]{1,0:T(8,128)(2,1)S(1)}, bf16[512,2048]{1,0:T(8,128)(2,1)}, u32[]{:S(2)}) copy-start(bf16[512,2048]{1,0:T(8,128)(2,1)} %get-tuple-element.51) | copy-start | bytes 6291460

commit v3 on v2

--- a/solution.py
+++ b/solution.py
@@ -13,7 +13,7 @@
 BF16 = jnp.bfloat16
 F32 = jnp.float32
 MESH = pl.DeviceIdType.MESH
-VMEM_LIMIT = 60 * 1024 * 1024
+VMEM_LIMIT = 28 * 1024 * 1024
 TN = ((0,), (0,))
 NN = ((1,), (0,))
 NT = ((1,), (1,))
@@ -117,11 +117,12 @@
     return before, after
 
 
-def dispatch_kernel(n, m, cap, q_ref, k_ref, v_ref, pre_ref, extra_ref, speed_ref, x_ref, cot_ref,
-                    pick_ref, comb_ref, gate_any, up_any, down_any,
+def dispatch_kernel(n, m, cap, q_any, k_any, v_any, pre_any, extra_any, speed_any, x_any, cot_any,
+                    pick_any, comb_any, gate_any, up_any, down_any,
                     rows_ref, hidden_ref, ggp_ref, gup_ref, place_ref, st_ref, cum_ref,
-                    normed_ref, inv_ref, mix_ref, carried_ref, last_ref,
-                    send_ref, sbuf, sin, lbuf, inner_ref, gate_v, up_v, down_v, gp_ref, up_ref,
+                    normed_ref, inv_ref, mix_ref, carried_ref, last_ref, gate_v, up_v,
+                    q_ref, k_ref, v_ref, pre_ref, speed_ref, cot_ref,
+                    extra_ref, x_ref, pick_ref, comb_ref, send_ref, sbuf, sin, lbuf, inner_ref, down_v, gp_ref, up_ref,
                     zs, zr, ys, yr, ps, pr, ss, sr, ws):
     at = Peers(n, m)
     me = at.me
@@ -129,12 +130,16 @@
     width = x_ref.shape[1]
     heads = channels // KEY_DIM
     slots = n * cap
-    at.greet()
-    loads = [pltpu.make_async_copy(src, dst, ws.at[i])
-             for i, (src, dst) in enumerate(((gate_any, gate_v), (up_any, up_v),
-                                             (down_any, down_v)))]
+    held = ((pick_any, pick_ref), (comb_any, comb_ref), (x_any, x_ref), (cot_any, cot_ref),
+            (pre_any, pre_ref), (extra_any, extra_ref), (speed_any, speed_ref), (q_any, q_ref),
+            (k_any, k_ref), (v_any, v_ref), (gate_any, gate_v), (up_any, up_v),
+            (down_any, down_v))
+    loads = [pltpu.make_async_copy(src, dst, ws.at[i]) for i, (src, dst) in enumerate(held)]
     for load in loads:
         load.start()
+    at.greet()
+    for load in loads[:4]:
+        load.wait()
 
     expert = lax.broadcasted_iota(jnp.int32, (n, tok), 0)
     picks = [pick_ref[i:i + 1, :] == expert for i in range(2)]
@@ -205,6 +210,9 @@
     for t in range(2):
         loop(n - 1, lambda i, t=t: out_row(t, i + 1).start())
 
+    for load in loads[4:10]:
+        load.wait()
+
     pre = pre_ref[...].astype(F32)
     log_sig = jnp.minimum(pre, 0.0) - jnp.log1p(jnp.exp(-jnp.abs(pre)))
     decays = as_column(speed_ref[...]) * log_sig + extra_ref[...]
@@ -269,10 +277,10 @@
             total = part if total is None else total + part
         return total
 
-    loads[0].wait()
+    loads[10].wait()
     gp_ref[...] = columns_of(gate_v, 0)
     loop(n - half, lambda d: pass_on(1, d + half))
-    loads[1].wait()
+    loads[11].wait()
     up_ref[...] = columns_of(up_v, 0)
     loop(n, lambda d: pass_mate(1, d))
 
@@ -293,7 +301,7 @@
         inv_ref[h * 8:(h + 1) * 8, :] = jnp.broadcast_to(inv, (8, tok))
 
     loop(n, lambda d: gathered(1, d))
-    loads[2].wait()
+    loads[12].wait()
     grad_hidden = None
     for j in range(m):
         part = dot(rows_ref[1, j], down_v[:, j * width:(j + 1) * width], NT)
@@ -322,6 +330,10 @@
     loop(n, drain_passed)
 
 
+def in_hbm(array):
+    return pltpu.with_memory_space_constraint(array, pltpu.HBM)
+
+
 def vmem_specs(count):
     return [pl.BlockSpec(memory_space=pltpu.VMEM)] * count
 
@@ -336,41 +348,40 @@
     outs = [((2, m, slots, width), BF16), ((slots, units), BF16), ((slots, units), BF16),
             ((slots, units), BF16), ((slots, tok), BF16), ((heads * tok, tok), BF16),
             ((channels, tok), F32), ((values, tok), F32), ((heads * 8, tok), F32),
-            ((values, tok), BF16), ((2, VAL_DIM, channels), F32), ((n, 8, channels), F32)]
+            ((values, tok), BF16), ((2, VAL_DIM, channels), F32), ((n, 8, channels), F32),
+            (gate.shape, BF16), (up.shape, BF16)]
+    outs += [(a.shape, a.dtype) for a in (q, k, v, pre, speed, cot)]
     return pl.pallas_call(
         functools.partial(dispatch_kernel, n, m, cap),
-        in_specs=vmem_specs(10) + [pl.BlockSpec(memory_space=pl.ANY)] * 3,
+        in_specs=[pl.BlockSpec(memory_space=pltpu.HBM)] * 13,
         out_specs=vmem_specs(len(outs)),
-        out_shape=[jax.ShapeDtypeStruct(shape, dtype) for shape, dtype in outs],
+        out_shape=[pltpu.VMEM(shape, dtype) for shape, dtype in outs],
         scratch_shapes=[
+            pltpu.VMEM(extra.shape, extra.dtype), pltpu.VMEM(x.shape, x.dtype),
+            pltpu.VMEM(picks.shape, picks.dtype), pltpu.VMEM(comb.shape, comb.dtype),
             pltpu.VMEM((2, slots, width), BF16), pltpu.VMEM((2, VAL_DIM, channels), BF16),
             pltpu.VMEM((n, VAL_DIM, channels), BF16), pltpu.VMEM((8, channels), F32),
             pltpu.VMEM((values, tok), F32),
-            pltpu.VMEM(gate.shape, BF16), pltpu.VMEM(up.shape, BF16), pltpu.VMEM(down.shape, BF16),
+            pltpu.VMEM(down.shape, BF16),
             pltpu.VMEM((slots, units), F32), pltpu.VMEM((slots, units), F32),
             dma((2, n)), dma((2, n)), dma((2, chips, n)), dma((2, chips, n)),
-            dma((2, chips, n)), dma((2, chips, n)), dma((2, n)), dma((2, n)), dma((3,)),
+            dma((2, chips, n)), dma((2, chips, n)), dma((2, n)), dma((2, n)), dma((13,)),
         ],
         compiler_params=pltpu.CompilerParams(collective_id=0, has_side_effects=True,
                                              vmem_limit_bytes=VMEM_LIMIT),
         name="dispatch",
-    )(q, k, v, pre, extra, speed, x, cot, picks, comb, gate, up, down)
+    )(*map(in_hbm, (q, k, v, pre, extra, speed, x, cot, picks, comb, gate, up, down)))
 
 
 def combine_kernel(n, m, cap, rows_ref, hidden_ref, ggp_ref, gup_ref, place_ref, cot_ref, mix_ref,
-                   gate_any, up_any,
+                   gate_v, up_v,
                    full_ref, dgate_ref, dup_ref, ddown_ref, all_mix_ref,
-                   gate_v, up_v, own_ref, psend, pin, ybuf, yin, zbuf, ret_ref,
-                   ps, pr, ys, yr, zs, zr, fs, fr, ms, mr, ws):
+                   own_ref, psend, pin, ybuf, yin, zbuf, ret_ref,
+                   ps, pr, ys, yr, zs, zr, fs, fr, ms, mr):
     at = Peers(n, m)
     me = at.me
     width = cot_ref.shape[1]
     at.greet()
-    loads = [pltpu.make_async_copy(src, dst, ws.at[i])
-             for i, (src, dst) in enumerate(((gate_any, gate_v), (up_any, up_v)))]
-    for load in loads:
-        load.start()
-
     def rows(p):
         return pl.ds(pl.multiple_of(p * cap, 16), cap)
 
@@ -410,8 +421,6 @@
         return copy_to(mix_ref, all_mix_ref.at[p], ms.at[d], mr.at[d], {"sp": p})
 
     all_mix_ref[me] = mix_ref[...]
-    loads[0].wait()
-    loads[1].wait()
     order = list(range(1, at.chips)) + [0]
     for i, dy in enumerate(order):
         psend[dy] = partial(column_of(dy, 1 - at.core)).astype(BF16)
@@ -514,17 +523,16 @@
             ((units, m * width), BF16), ((n,) + mix.shape, BF16)]
     return pl.pallas_call(
         functools.partial(combine_kernel, n, m, cap),
-        in_specs=vmem_specs(7) + [pl.BlockSpec(memory_space=pl.ANY)] * 2,
+        in_specs=vmem_specs(9),
         out_specs=vmem_specs(len(outs)),
-        out_shape=[jax.ShapeDtypeStruct(shape, dtype) for shape, dtype in outs],
+        out_shape=[pltpu.VMEM(shape, dtype) for shape, dtype in outs],
         scratch_shapes=[
-            pltpu.VMEM(gate.shape, BF16), pltpu.VMEM(up.shape, BF16),
             pltpu.VMEM((chips, slots, width), F32), pltpu.VMEM((chips, slots, width), BF16),
             pltpu.VMEM((chips, slots, width), BF16), pltpu.VMEM((chips, slots, width), BF16),
             pltpu.VMEM((chips, slots, width), BF16), pltpu.VMEM((slots, width), BF16),
             pltpu.VMEM((slots, width), BF16),
             dma((chips,)), dma((chips,)), dma((chips, n)), dma((chips, n)), dma((n,)), dma((n,)),
-            dma((2, chips)), dma((2, chips)), dma((n,)), dma((n,)), dma((2,)),
+            dma((2, chips)), dma((2, chips)), dma((n,)), dma((n,)),
         ],
         compiler_params=pltpu.CompilerParams(collective_id=1, has_side_effects=True,
                                              vmem_limit_bytes=VMEM_LIMIT),
@@ -732,12 +740,34 @@
         functools.partial(finish_kernel, n, m, project),
         in_specs=vmem_specs(len(args)),
         out_specs=vmem_specs(len(outs)),
-        out_shape=[jax.ShapeDtypeStruct(shape, dtype) for shape, dtype in outs],
+        out_shape=[pltpu.VMEM(shape, dtype) for shape, dtype in outs],
         scratch_shapes=scratch,
         compiler_params=pltpu.CompilerParams(collective_id=2, has_side_effects=True,
                                              vmem_limit_bytes=VMEM_LIMIT),
         name="finish",
     )(*args)
+
+
+def publish_kernel(*refs):
+    count = len(refs) // 2
+    sems = refs[-1]
+    copies = [pltpu.make_async_copy(refs[i], refs[count + i], sems.at[i]) for i in range(count)]
+    for copy in copies:
+        copy.start()
+    for copy in copies:
+        copy.wait()
+
+
+def publish(arrays):
+    return pl.pallas_call(
+        publish_kernel,
+        in_specs=vmem_specs(len(arrays)),
+        out_specs=[pl.BlockSpec(memory_space=pltpu.HBM)] * len(arrays),
+        out_shape=[jax.ShapeDtypeStruct(a.shape, a.dtype) for a in arrays],
+        scratch_shapes=[pltpu.SemaphoreType.DMA((len(arrays),))],
+        compiler_params=pltpu.CompilerParams(vmem_limit_bytes=1 << 20),
+        name="publish",
+    )(*[pltpu.with_memory_space_constraint(a, pltpu.VMEM) for a in arrays])
 
 
 def body(
@@ -764,38 +794,29 @@
     part_width = stored_expert_rows.shape[1]
     gate_local, up_local, down_local = expert_gate_weight[0], expert_up_weight[0], expert_down_weight[0]
     (rows, hidden, grad_gate_pre, grad_up_pre, place, scores, cum, normed, inv_rms, mix_rows,
-     carried, lasts) = dispatch(
+     carried, lasts, gate_held, up_held, q, k, v, pre, speed, cot) = dispatch(
         experts, m, capacity, queries, input_key_matrix, input_value_matrix,
         decay_preactivation, extra_log_decay, channel_decay_speed[None, :], stored_expert_rows,
         cotangent, chosen_expert_index.T, expert_combine_weight.T, gate_local, up_local, down_local)
     full, grad_gate, grad_up, grad_down, all_mix = combine(
-        experts, m, capacity, rows, hidden, grad_gate_pre, grad_up_pre, place, cotangent,
-        mix_rows, gate_local, up_local)
+        experts, m, capacity, rows, hidden, grad_gate_pre, grad_up_pre, place, cot,
+        mix_rows, gate_held, up_held)
     rows_block = output_weight_matrix.shape[0] // experts
     project = (tok_rows % (16 * m) == 0 and rows_block % 128 == 0
                and part_width % rows_block == 0)
     grads = finish(
-        experts, m, project, full, output_weight_matrix, normed, inv_rms, queries,
-        input_key_matrix, input_value_matrix, decay_preactivation, channel_decay_speed[None, :],
+        experts, m, project, full, output_weight_matrix, normed, inv_rms, q, k, v, pre, speed,
         cum, scores, carried, lasts, all_mix)
-    grad_queries, grad_keys, grad_values, grad_logit = grads[:4]
-    if project:
-        grad_out_proj = grads[4]
+    held = publish([*grads, grad_gate, grad_up, grad_down])
+    grad_gate, grad_up, grad_down = held[-3:]
+    if project:
+        grad_out_proj = held[4]
     else:
         full_rows = full.swapaxes(0, 1).reshape(tok_rows, experts, rows_block)
         all_rows = lax.all_to_all(full_rows.swapaxes(0, 1), "sp", split_axis=0, concat_axis=0,
                                   tiled=True)
         grad_out_proj = jnp.einsum("str,sct->rc", all_rows, all_mix, preferred_element_type=F32)
-    return (
-        grad_queries,
-        grad_keys,
-        grad_values,
-        grad_logit,
-        grad_out_proj,
-        grad_gate[None],
-        grad_up[None],
-        grad_down[None],
-    )
+    return (*held[:4], grad_out_proj, grad_gate[None], grad_up[None], grad_down[None])
 
 
 def solution(mesh):

time: 111 us -> 88.9 us (0.80)
  local copies, waits for them, and re-layouts: 13.7 us -> 0.01 us
  Pallas kernels: 96 us -> 87.9 us
    unnamed x14 -> x2, local copies, waits for them, and re-layouts: 13.7 us -> 0.01 us
    pallas_call x1, Pallas kernels: 38.6 us -> 33.8 us  [combine(): pl.pallas_call(functools.partial(combine_kernel, n, m, cap), in_specs=vme...]
    pallas_call x1, Pallas kernels: 21.3 us -> 18.5 us  [finish(): pl.pallas_call(functools.partial(finish_kernel, n, m, project), in_specs=...]
    pallas_call x1 -> x2, Pallas kernels: 36.1 us -> 35.6 us  [the longest x1 32.7 us: dispatch(): pl.pallas_call(functools.partial(dispatch_kernel, n, m, cap), in_specs=[p...]
where the time goes in v3:
time: 88.9 us; the launch traced here: 88.7 us
  Pallas kernels  87.9 us (99%)
    pallas_call x1, Pallas kernels, combine(): pl.pallas_call(functools.partial(combine_kernel, n, m, cap), in_specs=vme...  33.8 us
    pallas_call x1, Pallas kernels, dispatch(): pl.pallas_call(functools.partial(dispatch_kernel, n, m, cap), in_specs=[p...  32.7 us
    pallas_call x1, Pallas kernels, finish(): pl.pallas_call(functools.partial(finish_kernel, n, m, project), in_specs=...  18.5 us
    pallas_call x1, Pallas kernels, publish(): pl.pallas_call(publish_kernel, in_specs=vmem_specs(len(arrays)), out_spec...  2.97 us

profile of v3, /device:TPU:0, one launch (start us, length us, event | category | flops | bytes accessed | tf_op | source)
XLA Modules:
  0.0 88.7 jit_solution(5470814255936968145)
XLA Ops:
  0.6 32.7 %dispatch.1 = (bf16[2,4,384,512]{3,2,1,0:T(8,128)(2,1)S(1)}, bf16[384,512]{1,0:T(8,128)(2,1)S(1)}, bf16[384,512]{1,0:T(8,128)(2,1)S(1)}, bf16[384,512]{1,0:T(8,1...) custom-call(bf16[128,128]{1,0:T(8,128)(2,1)} %q_any.1, ...), custom_call_target="tpu_custom_call" | custom-call | tf_op jit(solution)/shard_map/dispatch/pallas_call | solution.py:354
  33.3 0.0 copy-start
  33.3 33.8 %combine.1 = (bf16[4,128,512]{2,1,0:T(8,128)(2,1)S(1)}, bf16[2048,512]{1,0:T(8,128)(2,1)S(1)}, bf16[2048,512]{1,0:T(8,128)(2,1)S(1)}, bf16[512,2048]{1,0:T(8,128)(2,1)S(1)}, bf16[8,256,128]{2,1,0:T(8,128)(2,1)S(1)}) custom-call(bf16[2,4,384,512]{3,2,1,0:T(8,128)(2,1)S(1)} %get-tuple-element.46.rows_ref, bf16[384,512]{1,0:T(8,128)(2,1)S(1)} %get-tuple-element.47.hidden_ref, ...), custom_call_target="tpu_custom_call" | custom-call | tf_op jit(solution)/shard_map/combine/pallas_call | solution.py:524
  67.1 0.0 copy-done
  67.1 18.5 %finish.1 = (f32[128,128]{1,0:T(8,128)S(1)}, f32[128,128]{1,0:T(8,128)S(1)}, f32[256,128]{1,0:T(8,128)S(1)}, f32[128,128]{1,0:T(8,128)S(1)}, f32[256,256]{1,0:T(8,128)S(1)}) custom-call(bf16[4,128,512]{2,1,0:T(8,128)(2,1)S(1)} %get-tuple-element.55.refs_0_, bf16[2048,256]{1,0:T(8,128)(2,1)S(1)} %copy-done, f32[256,128]{1,0:T(8,128)S(1)} %get-tuple-element.56.refs_2_, ...), custom_call_target="tpu_custom_call" | custom-call | tf_op jit(solution)/shard_map/finish/pallas_call | solution.py:739
  85.6 3.0 %publish.1 = (f32[128,128]{1,0:T(8,128)}, f32[128,128]{1,0:T(8,128)}, f32[256,128]{1,0:T(8,128)}, f32[128,128]{1,0:T(8,128)}, f32[256,256]{1,0:T(8,128)}, /*inde...) custom-call(f32[128,128]{1,0:T(8,128)S(1)} %get-tuple-element.68.refs_0_, ...), custom_call_target="tpu_custom_call" | custom-call | tf_op jit(solution)/shard_map/publish/pallas_call | solution.py:762
Async XLA Ops:
  33.3 33.8 %copy-start = (bf16[2048,256]{1,0:T(8,128)(2,1)S(1)}, bf16[2048,256]{1,0:T(8,128)(2,1)}, u32[]{:S(2)}) copy-start(bf16[2048,256]{1,0:T(8,128)(2,1)} %refs_1_.1) | copy-start | bytes 3145732
